TPU v7x, 32 devices: a whole 2x2x4 slice. The times are simulated.
32 devices in a mesh: sp: 8 (over z, y), tp: 4 (over x, core).
Axes of the slice: x: 2, y: 2, z: 4, core: 2. Of those that a mesh axis runs over, the one named last changes fastest.
Arguments:
- queries: bfloat16 [4096, 1024], P('sp', 'tp'), may hold values from -6 to 6
- keys: bfloat16 [4096, 1024], P('sp', 'tp'), may hold values from -6 to 6
- values: bfloat16 [4096, 1024], P('sp', 'tp'), may hold values from -6 to 6
- output_gate_logits: bfloat16 [4096, 1024], P('sp', 'tp'), may hold values from -6 to 6
- input_gate_log: float32 [4096, 8], P('sp', 'tp'), may hold values from -5 to 125
- forget_gate_logits: float32 [4096, 8], P('sp', 'tp')
- extra_decay_log: float32 [4096, 8], P('sp', 'tp'), may hold values from -1 to 0
- document: int32 [4096], P('sp'), may hold values from 0 to 3, never falling along the last dimension, each value on 1 to 2048 neighbouring positions
- residual: bfloat16 [4096, 2048], P('sp', 'tp'), may hold values from -16 to 16
- cell_norm_gain: bfloat16 [1024], P('tp'), may hold values from 0.099609375 to 1.8984375
- output_weight: bfloat16 [1024, 2048], P('tp'), may hold values from -0.1875 to 0.1875
- mixer_norm_gain: bfloat16 [2048], P('tp'), may hold values from 0.099609375 to 1.8984375
- up_weight: bfloat16 [2048, 8192], P('sp', 'tp'), may hold values from -0.125 to 0.125
- down_weight: bfloat16 [8192, 2048], P('tp', 'sp'), may hold values from -0.0625 to 0.0625
Outputs:
- layer_out: bfloat16 [4096, 2048], P('sp', 'tp')
All inputs are finite; a program needn't handle non-finite values.
Results may differ from a plain program's by a relative error of at most 0.015.
Values may be sent and summed in bfloat16 or wider, within the bound.
A program may use at most 128 MiB of HBM per device.

v0:
```python
import functools

import jax
import jax.numpy as jnp
from jax import lax
from jax.experimental import pallas as pl
from jax.experimental.pallas import tpu as pltpu
from jax.sharding import PartitionSpec as P

DH = 128
BLOCK = 128
MOST = 2048


NEG = -1e30
EPS = 1e-06
HIGH = lax.Precision.HIGHEST


def carried_in(value, axis, join, neutral):
    count, mine = (lax.axis_size(axis), lax.axis_index(axis))
    pieces = jax.tree.map(lambda part: lax.all_gather(part, axis), value)
    subtotal = jax.tree.map(
        lambda part, zero: jnp.full_like(part, 0) + jnp.asarray(zero, part.dtype), value, neutral
    )

    def step(position, subtotal):
        longer = join(subtotal, jax.tree.map(lambda part: part[position], pieces))
        return jax.tree.map(lambda new, old: jnp.where(position < mine, new, old), longer, subtotal)

    return lax.fori_loop(0, count - 1, step, subtotal)


def block_terms(carry, inputs):
    memory, normer, stabil, last_doc = carry
    q_blk, k_blk, v_blk, gate_in, gate_log, doc_blk = inputs
    length = doc_blk.shape[0]
    causal = jnp.arange(length)[:, None] >= jnp.arange(length)[None, :]
    cumulative = jnp.cumsum(gate_log, axis=-1)
    same_doc = (doc_blk[:, None] == doc_blk[None, :]) & causal
    pair_log = cumulative[:, :, None] - cumulative[:, None, :] + gate_in[:, None, :]
    pair_log = jnp.where(same_doc[None], pair_log, NEG)
    live_rows = doc_blk == last_doc
    carried_log = jnp.where(live_rows[None, :], cumulative + stabil[:, None], NEG)
    peak_log = jnp.maximum(carried_log, jnp.max(pair_log, axis=-1))
    weights = jnp.exp(pair_log - peak_log[:, :, None])
    carried = jnp.exp(carried_log - peak_log)
    scores = jnp.einsum("htd,hsd->hts", q_blk, k_blk, precision=HIGH) * weights
    numerator = carried[:, :, None] * jnp.einsum("htd,hde->hte", q_blk, memory, precision=HIGH)
    numerator = numerator + jnp.einsum("hts,hse->hte", scores, v_blk, precision=HIGH)
    denominator = carried * jnp.einsum("htd,hd->ht", q_blk, normer, precision=HIGH) + jnp.sum(
        scores, axis=-1
    )
    end_doc = doc_blk[-1]
    end_cum = cumulative[:, -1]
    keep_log = jnp.where(
        (doc_blk == end_doc)[None, :], end_cum[:, None] - cumulative + gate_in, NEG
    )
    old_log = jnp.where(last_doc == end_doc, end_cum + stabil, NEG)
    new_stab = jnp.maximum(old_log, jnp.max(keep_log, axis=-1))
    scaled = jnp.exp(keep_log - new_stab[:, None])
    decayed = jnp.exp(old_log - new_stab)
    memory = decayed[:, None, None] * memory + jnp.einsum(
        "hs,hsd,hse->hde", scaled, k_blk, v_blk, precision=HIGH
    )
    normer = decayed[:, None] * normer + jnp.einsum("hs,hsd->hd", scaled, k_blk, precision=HIGH)
    return ((memory, normer, new_stab, end_doc), (numerator, denominator, peak_log, cumulative))


def split_heads(source, blocks):
    return source.astype(jnp.float32).reshape(blocks, BLOCK, -1, DH).transpose(0, 2, 1, 3)


def split_gates(source, blocks):
    return source.reshape(blocks, BLOCK, -1).transpose(0, 2, 1)


def within_block_pass(
    queries, keys, values, input_gate_log, forget_gate_logits, extra_decay_log, document
):
    blocks = queries.shape[0] // BLOCK
    head_count = queries.shape[1] // DH
    query_heads = split_heads(queries, blocks) * DH ** (-0.5)
    forget_log_values = jax.nn.log_sigmoid(forget_gate_logits) + extra_decay_log
    inputs = (
        query_heads,
        split_heads(keys, blocks),
        split_heads(values, blocks),
        split_gates(input_gate_log, blocks),
        split_gates(forget_log_values, blocks),
        document.reshape(blocks, BLOCK),
    )
    initial = (
        jnp.zeros((head_count, DH, DH), jnp.float32),
        jnp.zeros((head_count, DH), jnp.float32),
        jnp.full((head_count,), NEG, jnp.float32),
        jnp.array(-1, jnp.int32),
    )
    final_state, output_rows = lax.scan(block_terms, initial, inputs)
    return (query_heads, final_state, output_rows)


def head_mix(cell_out, output_gate_logits, cell_norm_gain):
    row_count = output_gate_logits.shape[0]
    head_count = cell_out.shape[1]
    hidden = cell_out.transpose(0, 2, 1, 3).reshape(row_count, head_count * DH)
    squares = lax.psum(jnp.sum(hidden * hidden, axis=1), "tp")
    inverse = lax.rsqrt(squares / (head_count * DH * lax.axis_size("tp")) + EPS)
    gated = jax.nn.sigmoid(output_gate_logits.astype(jnp.float32))
    gains = cell_norm_gain.astype(jnp.float32)
    return (gated * hidden * inverse[:, None] * gains[None, :]).astype(jnp.bfloat16)


def join_states(earlier, later):
    mem_a, norm_a, stab_a, log_a, first_a, last_a = earlier
    mem_b, norm_b, stab_b, log_b, first_b, last_b = later
    joined = last_a == last_b
    stab_ab = jnp.where(joined, jnp.maximum(log_b + stab_a, stab_b), stab_b)
    weight_a = jnp.where(joined, jnp.exp(log_b + stab_a - stab_ab), 0.0)
    weight_b = jnp.exp(stab_b - stab_ab)
    memory = weight_a[:, None, None] * mem_a + weight_b[:, None, None] * mem_b
    normer = weight_a[:, None] * norm_a + weight_b[:, None] * norm_b
    blank_b = last_b < 0
    memory = jnp.where(blank_b, mem_a, memory)
    normer = jnp.where(blank_b, norm_a, normer)
    stabil = jnp.where(blank_b, stab_a, stab_ab)
    first_doc = jnp.where(first_a < 0, first_b, first_a)
    last_doc = jnp.where(blank_b, last_a, last_b)
    return (memory, normer, stabil, log_a + log_b, first_doc, last_doc)


def local(
    queries,
    keys,
    values,
    output_gate_logits,
    input_gate_log,
    forget_gate_logits,
    extra_decay_log,
    document,
    residual,
    cell_norm_gain,
    output_weight,
    mixer_norm_gain,
    up_weight,
    down_weight,
):
    query_heads, final_state, output_rows = within_block_pass(
        queries, keys, values, input_gate_log, forget_gate_logits, extra_decay_log, document
    )
    numerator, denominator, peak_log, cumulative = output_rows
    memory, normer, stabil, last_doc = final_state
    step_logs = cumulative[:, :, -1]
    offsets = jnp.cumsum(step_logs, axis=0) - step_logs
    through = cumulative + offsets[:, :, None]
    summary = (memory, normer, stabil, jnp.sum(step_logs, axis=0), document[0], last_doc)
    identity = (
        jnp.zeros_like(memory),
        jnp.zeros_like(normer),
        jnp.full_like(stabil, NEG),
        jnp.zeros_like(stabil),
        jnp.array(-1, jnp.int32),
        jnp.array(-1, jnp.int32),
    )
    prefix = carried_in(summary, "sp", join_states, identity)
    doc_blocks = document.reshape(-1, BLOCK)
    carried_log = jnp.where(
        (doc_blocks == prefix[5])[:, None, :], through + prefix[2][None, :, None], NEG
    )
    merged_peak = jnp.maximum(peak_log, carried_log)
    own_weight = jnp.exp(peak_log - merged_peak)
    far_weight = jnp.exp(carried_log - merged_peak)
    numerator = own_weight[..., None] * numerator + far_weight[..., None] * jnp.einsum(
        "nhtd,hde->nhte", query_heads, prefix[0], precision=HIGH
    )
    denominator = own_weight * denominator + far_weight * jnp.einsum(
        "nhtd,hd->nht", query_heads, prefix[1], precision=HIGH
    )
    cell_out = numerator / jnp.maximum(jnp.abs(denominator), 1.0)[..., None]
    mixed = head_mix(cell_out, output_gate_logits, cell_norm_gain)
    head_terms = jnp.dot(mixed, output_weight, preferred_element_type=jnp.float32)
    width = residual.shape[1]
    model_width = width * lax.axis_size("tp")
    own_sum = lax.psum_scatter(
        head_terms.astype(jnp.bfloat16), "tp", scatter_dimension=1, tiled=True
    ).astype(jnp.float32)
    first_sum = (residual.astype(jnp.float32) + own_sum).astype(jnp.bfloat16)
    first_wide = lax.optimization_barrier(first_sum).astype(jnp.float32)
    squares = lax.psum(jnp.sum(first_wide * first_wide, axis=1), "tp")
    inverse = lax.rsqrt(squares / model_width + EPS)
    normed_own = (first_wide * inverse[:, None] * mixer_norm_gain.astype(jnp.float32)).astype(
        jnp.bfloat16
    )
    normed_full = lax.all_gather(normed_own, "tp", axis=1, tiled=True)
    hidden = jnp.dot(
        normed_full,
        lax.all_gather(up_weight, "sp", axis=0, tiled=True),
        preferred_element_type=jnp.float32,
    )
    squared = jnp.square(jax.nn.relu(hidden)).astype(jnp.bfloat16)
    channel = jnp.dot(
        squared,
        lax.all_gather(down_weight, "sp", axis=1, tiled=True),
        preferred_element_type=jnp.float32,
    )
    own_channel = lax.psum_scatter(
        channel.astype(jnp.bfloat16), "tp", scatter_dimension=1, tiled=True
    ).astype(jnp.float32)
    return (lax.optimization_barrier(first_sum).astype(jnp.float32) + own_channel).astype(
        jnp.bfloat16
    )


MESH = pl.DeviceIdType.MESH
F32 = jnp.float32
BF16 = jnp.bfloat16


def to_columns(rows):
    pad = jnp.zeros((128 - rows.shape[0], rows.shape[1]), F32)
    return jnp.transpose(jnp.concatenate([rows, pad], axis=0))


def row_sums(wide):
    ones = jnp.ones((8, wide.shape[1]), F32)
    return lax.dot_general(
        ones, wide, (((1,), (1,)), ((), ())), precision=HIGH, preferred_element_type=F32
    )


def layer_kernel(
    n,
    m,
    back,
    q_ref,
    k_ref,
    v_ref,
    og_ref,
    gates_ref,
    resid_ref,
    gain_ref,
    wout_ref,
    up_ref,
    down_ref,
    out_ref,
    up_all,
    down_all,
    state_out,
    state_in,
    tail_out,
    tail_in,
    y_ref,
    terms_out,
    terms_in,
    squares_out,
    squares_in,
    first_ref,
    normed,
    sums_out,
    sums_in,
    squared,
    parts_out,
    parts_in,
    ring_send,
    ring_recv,
    state_send,
    state_recv,
    tail_send,
    tail_recv,
    terms_send,
    terms_recv,
    squares_send,
    squares_recv,
    normed_send,
    normed_recv,
    sums_send,
    sums_recv,
    parts_send,
    parts_recv,
):
    sp, tp = lax.axis_index("sp"), lax.axis_index("tp")
    rows, heads = q_ref.shape[0], q_ref.shape[1] // DH
    depth, hidden_width = up_ref.shape
    half, quarter = depth // 2, depth // 4
    width = resid_ref.shape[1]
    per_owner = width // depth

    def index_of(position):
        late = position // (n // 2)
        return (1 - late) * 2 * position + late * (2 * (n - 1 - position) + 1)

    odd = sp % 2
    place = (1 - odd) * (sp // 2) + odd * (n - 1 - sp // 2)
    target = (index_of((place + 1) % n), index_of((place + n - 1) % n))

    barrier = pltpu.get_barrier_semaphore()
    for k in range(1, n):
        pl.semaphore_signal(barrier, device_id=((sp + k) % n, tp), device_id_type=MESH)
    for k in range(1, m):
        pl.semaphore_signal(barrier, device_id=(sp, (tp + k) % m), device_id_type=MESH)
    pl.semaphore_wait(barrier, n + m - 2)

    def block_at(way, step):
        return index_of((place + (n - step if way == 0 else step)) % n)

    def ring(stream, way, step, sub):
        block = block_at(way, step)
        if stream == 0:
            inner = way * half + sub * quarter
            where = pl.ds(pl.multiple_of(block * depth + inner, quarter), quarter)
            dst = up_all.at[where, :]
            src = up_ref.at[pl.ds(inner, quarter), :] if step == 0 else dst
        else:
            deep = pl.ds(sub * (hidden_width // 2), hidden_width // 2)
            dst = down_all.at[block, way, deep, :]
            src = down_ref.at[deep, pl.ds(way * half, half)] if step == 0 else dst
        return pltpu.make_async_remote_copy(
            src_ref=src,
            dst_ref=dst,
            send_sem=ring_send.at[stream, way, step, sub],
            recv_sem=ring_recv.at[stream, way, step, sub],
            device_id=(target[way], tp),
            device_id_type=MESH,
        )

    def arrived(stream, way, step, sub):
        block = block_at(way, step + 1)
        if stream == 0:
            inner = way * half + sub * quarter
            dst = up_all.at[pl.ds(pl.multiple_of(block * depth + inner, quarter), quarter), :]
        else:
            dst = down_all.at[block, way, pl.ds(sub * (hidden_width // 2), hidden_width // 2), :]
        pltpu.make_async_remote_copy(
            src_ref=dst,
            dst_ref=dst,
            send_sem=ring_send.at[stream, way, step, sub],
            recv_sem=ring_recv.at[stream, way, step, sub],
            device_id=(target[way], tp),
            device_id_type=MESH,
        ).wait_recv()

    def open_stream(stream, sub):
        for way in range(2):
            ring(stream, way, 0, sub).start()

    events = [(a, b, c) for a in range(2) for b in range(n - 1) for c in range(2)]
    done = [0]

    def pump():
        stream, step, sub = events[done[0]]
        done[0] += 1
        for way in range(2):
            arrived(stream, way, step, sub)
            if step + 1 < n - 1:
                ring(stream, way, step + 1, sub).start()
        if stream == 0 and step == n - 2:
            open_stream(1, sub)

    open_stream(0, 0)

    gates = gates_ref[...]
    document = gates[2 * heads : 2 * heads + 1, :]
    across = lax.broadcasted_iota(jnp.int32, (rows, rows), 1)
    along = lax.broadcasted_iota(jnp.int32, (rows, rows), 0)
    upper = (along <= across).astype(F32)
    sums = jnp.dot(gates, upper, precision=HIGH, preferred_element_type=F32)
    last_doc = document[:, rows - 1 : rows]
    totals, stabs, scaled = [], [], []
    for h in range(heads):
        total = sums[h : h + 1, rows - 1 : rows]
        keep = total - sums[h : h + 1, :] + gates[heads + h : heads + h + 1, :]
        keep = jnp.where(document == last_doc, keep, NEG)
        stab = jnp.max(keep, axis=1, keepdims=True)
        totals.append(total)
        stabs.append(stab)
        scaled.append(jnp.exp(keep - stab))
    slab = lax.broadcasted_iota(jnp.int32, (8, rows), 0)
    packed = jnp.broadcast_to(document, (8, rows))
    for h in range(heads):
        packed = jnp.where(slab == h, sums[h : h + 1, :], packed)
        packed = jnp.where(slab == heads + h, scaled[h], packed)
    columns = to_columns(packed)
    doc_col = columns[:, 2 * heads : 2 * heads + 1]
    line = lax.broadcasted_iota(jnp.int32, (8, DH), 0)
    for h in range(heads):
        mine = slice(h * DH, (h + 1) * DH)
        weighted = k_ref[:, mine].astype(F32) * columns[:, heads + h : heads + h + 1]
        state_out[h] = jnp.dot(
            jnp.transpose(weighted),
            v_ref[:, mine].astype(F32),
            precision=HIGH,
            preferred_element_type=F32,
        ).astype(BF16)
        tail = jnp.broadcast_to(jnp.sum(weighted, axis=0, keepdims=True), (8, DH))
        tail = jnp.where(line == 1, stabs[h], tail)
        tail = jnp.where(line == 2, totals[h], tail)
        tail = jnp.where(line == 3, last_doc, tail)
        tail_out[h] = tail

    def state_copies(k):
        return [
            pltpu.make_async_remote_copy(
                src_ref=src,
                dst_ref=dst.at[k - 1],
                send_sem=send_sem.at[k - 1],
                recv_sem=recv_sem.at[k - 1],
                device_id=((sp + k) % n, tp),
                device_id_type=MESH,
            )
            for src, dst, send_sem, recv_sem in (
                (tail_out, tail_in, tail_send, tail_recv),
                (state_out, state_in, state_send, state_recv),
            )
        ]

    for k in range(1, back + 1):

        @pl.when(sp + k < n)
        def _():
            for copy in state_copies(k):
                copy.start()

        @pl.when(sp < k)
        def _():
            tail_in[k - 1] = jnp.zeros((heads, 8, DH), F32)
            state_in[k - 1] = jnp.zeros((heads, DH, DH), BF16)

    open_stream(0, 1)

    own_rows = pl.ds(pl.multiple_of(sp * depth, depth), depth)
    up_all[own_rows, :] = up_ref[...]
    down_all[sp, 0] = down_ref[:, 0:half]
    down_all[sp, 1] = down_ref[:, half:depth]
    pump()

    locals_of = []
    for h in range(heads):
        mine = slice(h * DH, (h + 1) * DH)
        scores = lax.dot_general(
            q_ref[:, mine],
            k_ref[:, mine],
            (((1,), (1,)), ((), ())),
            preferred_element_type=F32,
        ) * (DH**-0.5)
        pair = columns[:, h : h + 1] - sums[h : h + 1, :] + gates[heads + h : heads + h + 1, :]
        pair = jnp.where((doc_col == document) & (along >= across), pair, NEG)
        peak = jnp.max(pair, axis=1, keepdims=True)
        scores = scores * jnp.exp(pair - peak)
        numer = jnp.dot(
            scores, v_ref[:, mine].astype(F32), precision=HIGH, preferred_element_type=F32
        )
        locals_of.append((peak, jnp.sum(scores, axis=1, keepdims=True), numer))
        pump()

    for k in range(1, back + 1):

        @pl.when(sp >= k)
        def _():
            for copy in state_copies(k):
                copy.wait_recv()

    first_doc = document[:, 0:1]
    cells = []
    for h in range(heads):
        mine = slice(h * DH, (h + 1) * DH)
        between = jnp.zeros((1, DH), F32)
        logs, valids = [], []
        best = jnp.full((1, DH), NEG, F32)
        for k in range(1, back + 1):
            tail = tail_in[k - 1, h]
            far = lax.broadcasted_iota(jnp.int32, (1, DH), 1) * 0 + sp
            valid = (tail[3:4, :] == first_doc) & (far >= k)
            log = jnp.where(valid, between + tail[1:2, :], NEG)
            between = between + tail[2:3, :]
            best = jnp.maximum(best, log)
            logs.append(log)
            valids.append(valid)
        memory = jnp.zeros((DH, DH), F32)
        normer = jnp.zeros((1, DH), F32)
        for k in range(1, back + 1):
            weight = jnp.where(valids[k - 1], jnp.exp(logs[k - 1] - best), 0.0)
            memory = memory + jnp.where(
                valids[k - 1], weight * state_in[k - 1, h].astype(F32), 0.0
            )
            normer = normer + jnp.where(
                valids[k - 1], weight * tail_in[k - 1, h, 0:1, :], 0.0
            )
        peak, denom, numer = locals_of[h]
        carried = jnp.where(doc_col == first_doc, columns[:, h : h + 1] + best[:, 0:1], NEG)
        merged = jnp.maximum(peak, carried)
        own, other = jnp.exp(peak - merged), jnp.exp(carried - merged)
        query = q_ref[:, mine].astype(F32) * (DH**-0.5)
        numer = own * numer + other * jnp.dot(
            query, memory, precision=HIGH, preferred_element_type=F32
        )
        denom = own * denom + other * jnp.sum(query * normer, axis=1, keepdims=True)
        cell = numer / jnp.maximum(jnp.abs(denom), 1.0)
        cells.append(cell)
        gated = jax.nn.sigmoid(og_ref[:, mine].astype(F32))
        y_ref[:, mine] = (gated * cell * gain_ref[:, mine].astype(F32)).astype(BF16)
    total = cells[0] * cells[0]
    for h in range(1, heads):
        total = total + cells[h] * cells[h]
    squares_out[...] = row_sums(total)

    def to_peer(src, dst, send_sem, recv_sem, k):
        return pltpu.make_async_remote_copy(
            src_ref=src,
            dst_ref=dst,
            send_sem=send_sem.at[k - 1],
            recv_sem=recv_sem.at[k - 1],
            device_id=(sp, (tp + k) % m),
            device_id_type=MESH,
        )

    def squares_copy(k):
        return to_peer(squares_out, squares_in.at[k - 1], squares_send, squares_recv, k)

    def terms_copy(k):
        return to_peer(terms_out.at[k], terms_in.at[k - 1], terms_send, terms_recv, k)

    def head_term(k):
        owner = (tp + k) % m
        cols = pl.ds(pl.multiple_of(owner * width, width), width)
        return jnp.dot(y_ref[...], wout_ref[:, cols], preferred_element_type=F32).astype(BF16)

    for k in range(1, m):
        squares_copy(k).start()
        terms_out[k] = head_term(k)
        terms_copy(k).start()
    own_term = head_term(0).astype(F32)
    terms_out[0] = own_term.astype(BF16)
    for _ in range(min(PUMPS_TERMS, 2 * (n - 1) - done[0])):
        pump()
    for k in range(1, m):
        squares_copy(k).wait_recv()
        terms_copy(k).wait_recv()
    squares = squares_out[...]
    attn = terms_out[0].astype(F32)
    for k in range(1, m):
        squares = squares + squares_in[k - 1]
        attn = attn + terms_in[k - 1].astype(F32)
    inverse = lax.rsqrt(to_columns(squares)[:, 0:1] / (heads * DH * m) + EPS)
    first = (resid_ref[...].astype(F32) + attn * inverse).astype(BF16)
    first_ref[...] = first
    first = first.astype(F32)
    here = pl.ds(pl.multiple_of(tp * width, width), width)
    normed[:, here] = (first * gain_ref[:, heads * DH :].astype(F32)).astype(BF16)
    sums_out[...] = row_sums(first * first)

    def normed_copy(k):
        return to_peer(normed.at[:, here], normed.at[:, here], normed_send, normed_recv, k)

    def normed_arrival(k):
        source = (tp + m - k) % m
        there = normed.at[:, pl.ds(pl.multiple_of(source * width, width), width)]
        return to_peer(there, there, normed_send, normed_recv, k)

    def sums_copy(k):
        return to_peer(sums_out, sums_in.at[k - 1], sums_send, sums_recv, k)

    for k in range(1, m):
        sums_copy(k).start()
        normed_copy(k).start()
    while done[0] < 2 * (n - 1):
        pump()
    for k in range(1, m):
        sums_copy(k).wait_recv()
        normed_arrival(k).wait_recv()
    squares = sums_out[...]
    for k in range(1, m):
        squares = squares + sums_in[k - 1]
    scale = lax.rsqrt(to_columns(squares)[:, 0:1] / (width * m) + EPS)

    tile = min(hidden_width, 256)
    chunks = hidden_width // tile

    def up_chunk(c, carry):
        cols = pl.ds(pl.multiple_of(c * tile, tile), tile)
        raw = jnp.dot(normed[...], up_all[:, cols], preferred_element_type=F32)
        hidden = jnp.maximum(raw * scale, 0.0)
        squared[:, cols] = (hidden * hidden).astype(BF16)
        return carry

    lax.fori_loop(0, chunks // 2, up_chunk, 0)
    pump()
    lax.fori_loop(chunks // 2, chunks, up_chunk, 0)

    def part_copy(way, step):
        block = block_at(way, step)
        owner, slot = block // per_owner, block % per_owner
        return owner, pltpu.make_async_remote_copy(
            src_ref=parts_out.at[block, way],
            dst_ref=parts_in.at[tp, slot, way],
            send_sem=parts_send.at[block, way],
            recv_sem=parts_recv.at[tp, slot, way],
            device_id=(sp, owner),
            device_id_type=MESH,
        )

    def down_block(step):
        for way in range(2):
            block = block_at(way, step)
            parts_out[block, way] = jnp.dot(
                squared[...], down_all[block, way], preferred_element_type=F32
            ).astype(BF16)
            owner, copy = part_copy(way, step)

            @pl.when(owner != tp)
            def _():
                copy.start()

    down_block(0)
    for step in range(1, n):
        while done[0] < 2 * (n - 1) + 2 * step:
            pump()
        down_block(step)

    for slot in range(per_owner):
        for way in range(2):
            cols = slice(slot * depth + way * half, slot * depth + (way + 1) * half)
            total = parts_out[tp * per_owner + slot, way].astype(F32)
            for k in range(1, m):
                source = (tp + k) % m
                there = parts_in.at[source, slot, way]
                pltpu.make_async_remote_copy(
                    src_ref=there,
                    dst_ref=there,
                    send_sem=parts_send.at[0, 0],
                    recv_sem=parts_recv.at[source, slot, way],
                    device_id=(sp, source),
                    device_id_type=MESH,
                ).wait_recv()
                total = total + parts_in[source, slot, way].astype(F32)
            out_ref[:, cols] = (first_ref[:, cols].astype(F32) + total).astype(BF16)

    for stream, step, sub in events:
        for way in range(2):
            ring(stream, way, step, sub).wait_send()
    for k in range(1, back + 1):

        @pl.when(sp + k < n)
        def _():
            for copy in state_copies(k):
                copy.wait_send()

    for k in range(1, m):
        squares_copy(k).wait_send()
        terms_copy(k).wait_send()
        sums_copy(k).wait_send()
        normed_copy(k).wait_send()
    for step in range(n):
        for way in range(2):
            owner, copy = part_copy(way, step)

            @pl.when(owner != tp)
            def _():
                copy.wait_send()


PUMPS_TERMS = 5


def fused(
    n,
    m,
    queries,
    keys,
    values,
    output_gate_logits,
    input_gate_log,
    forget_gate_logits,
    extra_decay_log,
    document,
    residual,
    cell_norm_gain,
    output_weight,
    mixer_norm_gain,
    up_weight,
    down_weight,
):
    rows, heads = queries.shape[0], queries.shape[1] // DH
    depth, hidden_width = up_weight.shape
    width = residual.shape[1]
    back = min(n - 1, (MOST - 2) // rows + 1)
    forget = jax.nn.log_sigmoid(forget_gate_logits) + extra_decay_log
    gates = jnp.concatenate(
        [forget.T, input_gate_log.T, document.astype(F32)[None, :]], axis=0
    )
    gates = jnp.pad(gates, ((0, 8 - gates.shape[0]), (0, 0)))
    dma = pltpu.SemaphoreType.DMA
    per_owner = width // depth
    return pl.pallas_call(
        functools.partial(layer_kernel, n, m, back),
        out_shape=jax.ShapeDtypeStruct((rows, width), BF16),
        in_specs=[pl.BlockSpec(memory_space=pltpu.VMEM)] * 10,
        out_specs=pl.BlockSpec(memory_space=pltpu.VMEM),
        scratch_shapes=[
            pltpu.VMEM((n * depth, hidden_width), BF16),
            pltpu.VMEM((n, 2, hidden_width, depth // 2), BF16),
            pltpu.VMEM((heads, DH, DH), BF16),
            pltpu.VMEM((back, heads, DH, DH), BF16),
            pltpu.VMEM((heads, 8, DH), F32),
            pltpu.VMEM((back, heads, 8, DH), F32),
            pltpu.VMEM((rows, heads * DH), BF16),
            pltpu.VMEM((m, rows, width), BF16),
            pltpu.VMEM((m - 1, rows, width), BF16),
            pltpu.VMEM((8, rows), F32),
            pltpu.VMEM((m - 1, 8, rows), F32),
            pltpu.VMEM((rows, width), BF16),
            pltpu.VMEM((rows, m * width), BF16),
            pltpu.VMEM((8, rows), F32),
            pltpu.VMEM((m - 1, 8, rows), F32),
            pltpu.VMEM((rows, hidden_width), BF16),
            pltpu.VMEM((n, 2, rows, depth // 2), BF16),
            pltpu.VMEM((m, per_owner, 2, rows, depth // 2), BF16),
            dma((2, 2, n - 1, 2)),
            dma((2, 2, n - 1, 2)),
            dma((back,)),
            dma((back,)),
            dma((back,)),
            dma((back,)),
            dma((m - 1,)),
            dma((m - 1,)),
            dma((m - 1,)),
            dma((m - 1,)),
            dma((m - 1,)),
            dma((m - 1,)),
            dma((m - 1,)),
            dma((m - 1,)),
            dma((n, 2)),
            dma((m, per_owner, 2)),
        ],
        compiler_params=pltpu.CompilerParams(
            collective_id=0, has_side_effects=True, vmem_limit_bytes=60 * 1024 * 1024
        ),
        name="layer",
    )(
        queries,
        keys,
        values,
        output_gate_logits,
        gates,
        residual,
        jnp.concatenate([cell_norm_gain, mixer_norm_gain])[None, :],
        output_weight,
        up_weight,
        down_weight,
    )


def either(n, m, *args):
    depth, hidden_width = args[12].shape
    heads = args[0].shape[1] // DH
    fits = depth % 256 == 0 and n % 2 == 0 and n >= 4 and n <= 16 and m >= 2
    fits = fits and 2 * heads + 1 <= 8 and args[8].shape[1] % depth == 0
    fits = fits and args[0].shape[0] % 128 == 0 and hidden_width % 256 == 0
    if fits:
        return fused(n, m, *args)
    return local(*args)


def solution(mesh):
    in_specs = (
        P("sp", "tp"),
        P("sp", "tp"),
        P("sp", "tp"),
        P("sp", "tp"),
        P("sp", "tp"),
        P("sp", "tp"),
        P("sp", "tp"),
        P("sp"),
        P("sp", "tp"),
        P("tp"),
        P("tp", None),
        P("tp"),
        P("sp", "tp"),
        P("tp", "sp"),
    )
    out_specs = P("sp", "tp")
    body = functools.partial(either, mesh.shape["sp"], mesh.shape["tp"])
    return jax.shard_map(body, mesh=mesh, in_specs=in_specs, out_specs=out_specs, check_vma=False)
```

profile of v0, /device:TPU:23, one launch (start us, length us, event | category | flops | bytes accessed | tf_op | source)
XLA Modules:
  0.0 186.5 jit_solution(10357814967647482060)
XLA Ops:
  0.0 0.7 convert_element_type.5
  0.7 0.0 copy-start.3
  0.7 0.0 copy-start.4
  0.7 0.7 copy-done.3
  1.4 0.0 copy-done.4
  1.4 0.0 copy-start
  1.4 0.0 copy-start.1
  1.4 0.6 broadcast_in_dim.7.gain_ref
  2.0 0.1 copy-done
  2.1 0.0 copy-done.1
  2.1 0.0 copy-start.2
  2.1 0.7 copy-done.2
  2.8 0.6 select_maximum_fusion.gates_ref
  3.4 181.2 %layer.1 = bf16[512,512]{1,0:T(8,128)(2,1)} custom-call(bf16[512,256]{1,0:T(8,128)(2,1)} %q_ref.1, bf16[512,256]{1,0:T(8,128)(2,1)} %k_ref.1, bf16[512,256]{1,0:T(8,128)(2,1)} %v_ref.1, bf16[512,256]{1,0:T(8,128)(2,1)} %og_ref.1, f32[8,512]{1,0:T(8,128)} %select_maximum_fusion.gates_ref, bf16[512,512]{1,0:T(8,128)(2,1)} %resid_ref.1, ...), custom_call_target="tpu_custom_call" | custom-call | tf_op jit(solution)/shard_map/layer/pallas_call | solution.py:693
  184.6 1.9 %copy.16 = bf16[512,512]{1,0:T(8,128)(2,1)} copy(bf16[512,512]{1,0:T(8,128)(2,1)} %layer.1) | data formatting | bytes 1048576
  (2 shorter events, 0.0 us)
Async XLA Ops:
  0.7 0.7 copy-start.3
  0.7 0.7 copy-start.4
  1.4 0.7 copy-start
  1.4 0.7 copy-start.1
  2.1 0.7 copy-start.2
where the time goes:
time: 187 us; the launch traced here: 186 us
  Pallas kernels  181 us (97%)
  local copies, waits for them, and re-layouts  3.9 us (2%)
    pallas_call x1, Pallas kernels, fused(): pl.pallas_call(functools.partial(layer_kernel, n, m, back), out_shape=jax...  181 us

commit v1 on v0

v1 whole, which is shorter than its diff:
```python
import functools

import jax
import jax.numpy as jnp
from jax import lax
from jax.experimental import pallas as pl
from jax.experimental.pallas import tpu as pltpu
from jax.sharding import PartitionSpec as P

DH = 128
BLOCK = 128
MOST = 2048


NEG = -1e30
EPS = 1e-06
HIGH = lax.Precision.HIGHEST


def carried_in(value, axis, join, neutral):
    count, mine = (lax.axis_size(axis), lax.axis_index(axis))
    pieces = jax.tree.map(lambda part: lax.all_gather(part, axis), value)
    subtotal = jax.tree.map(
        lambda part, zero: jnp.full_like(part, 0) + jnp.asarray(zero, part.dtype), value, neutral
    )

    def step(position, subtotal):
        longer = join(subtotal, jax.tree.map(lambda part: part[position], pieces))
        return jax.tree.map(lambda new, old: jnp.where(position < mine, new, old), longer, subtotal)

    return lax.fori_loop(0, count - 1, step, subtotal)


def block_terms(carry, inputs):
    memory, normer, stabil, last_doc = carry
    q_blk, k_blk, v_blk, gate_in, gate_log, doc_blk = inputs
    length = doc_blk.shape[0]
    causal = jnp.arange(length)[:, None] >= jnp.arange(length)[None, :]
    cumulative = jnp.cumsum(gate_log, axis=-1)
    same_doc = (doc_blk[:, None] == doc_blk[None, :]) & causal
    pair_log = cumulative[:, :, None] - cumulative[:, None, :] + gate_in[:, None, :]
    pair_log = jnp.where(same_doc[None], pair_log, NEG)
    live_rows = doc_blk == last_doc
    carried_log = jnp.where(live_rows[None, :], cumulative + stabil[:, None], NEG)
    peak_log = jnp.maximum(carried_log, jnp.max(pair_log, axis=-1))
    weights = jnp.exp(pair_log - peak_log[:, :, None])
    carried = jnp.exp(carried_log - peak_log)
    scores = jnp.einsum("htd,hsd->hts", q_blk, k_blk, precision=HIGH) * weights
    numerator = carried[:, :, None] * jnp.einsum("htd,hde->hte", q_blk, memory, precision=HIGH)
    numerator = numerator + jnp.einsum("hts,hse->hte", scores, v_blk, precision=HIGH)
    denominator = carried * jnp.einsum("htd,hd->ht", q_blk, normer, precision=HIGH) + jnp.sum(
        scores, axis=-1
    )
    end_doc = doc_blk[-1]
    end_cum = cumulative[:, -1]
    keep_log = jnp.where(
        (doc_blk == end_doc)[None, :], end_cum[:, None] - cumulative + gate_in, NEG
    )
    old_log = jnp.where(last_doc == end_doc, end_cum + stabil, NEG)
    new_stab = jnp.maximum(old_log, jnp.max(keep_log, axis=-1))
    scaled = jnp.exp(keep_log - new_stab[:, None])
    decayed = jnp.exp(old_log - new_stab)
    memory = decayed[:, None, None] * memory + jnp.einsum(
        "hs,hsd,hse->hde", scaled, k_blk, v_blk, precision=HIGH
    )
    normer = decayed[:, None] * normer + jnp.einsum("hs,hsd->hd", scaled, k_blk, precision=HIGH)
    return ((memory, normer, new_stab, end_doc), (numerator, denominator, peak_log, cumulative))


def split_heads(source, blocks):
    return source.astype(jnp.float32).reshape(blocks, BLOCK, -1, DH).transpose(0, 2, 1, 3)


def split_gates(source, blocks):
    return source.reshape(blocks, BLOCK, -1).transpose(0, 2, 1)


def within_block_pass(
    queries, keys, values, input_gate_log, forget_gate_logits, extra_decay_log, document
):
    blocks = queries.shape[0] // BLOCK
    head_count = queries.shape[1] // DH
    query_heads = split_heads(queries, blocks) * DH ** (-0.5)
    forget_log_values = jax.nn.log_sigmoid(forget_gate_logits) + extra_decay_log
    inputs = (
        query_heads,
        split_heads(keys, blocks),
        split_heads(values, blocks),
        split_gates(input_gate_log, blocks),
        split_gates(forget_log_values, blocks),
        document.reshape(blocks, BLOCK),
    )
    initial = (
        jnp.zeros((head_count, DH, DH), jnp.float32),
        jnp.zeros((head_count, DH), jnp.float32),
        jnp.full((head_count,), NEG, jnp.float32),
        jnp.array(-1, jnp.int32),
    )
    final_state, output_rows = lax.scan(block_terms, initial, inputs)
    return (query_heads, final_state, output_rows)


def head_mix(cell_out, output_gate_logits, cell_norm_gain):
    row_count = output_gate_logits.shape[0]
    head_count = cell_out.shape[1]
    hidden = cell_out.transpose(0, 2, 1, 3).reshape(row_count, head_count * DH)
    squares = lax.psum(jnp.sum(hidden * hidden, axis=1), "tp")
    inverse = lax.rsqrt(squares / (head_count * DH * lax.axis_size("tp")) + EPS)
    gated = jax.nn.sigmoid(output_gate_logits.astype(jnp.float32))
    gains = cell_norm_gain.astype(jnp.float32)
    return (gated * hidden * inverse[:, None] * gains[None, :]).astype(jnp.bfloat16)


def join_states(earlier, later):
    mem_a, norm_a, stab_a, log_a, first_a, last_a = earlier
    mem_b, norm_b, stab_b, log_b, first_b, last_b = later
    joined = last_a == last_b
    stab_ab = jnp.where(joined, jnp.maximum(log_b + stab_a, stab_b), stab_b)
    weight_a = jnp.where(joined, jnp.exp(log_b + stab_a - stab_ab), 0.0)
    weight_b = jnp.exp(stab_b - stab_ab)
    memory = weight_a[:, None, None] * mem_a + weight_b[:, None, None] * mem_b
    normer = weight_a[:, None] * norm_a + weight_b[:, None] * norm_b
    blank_b = last_b < 0
    memory = jnp.where(blank_b, mem_a, memory)
    normer = jnp.where(blank_b, norm_a, normer)
    stabil = jnp.where(blank_b, stab_a, stab_ab)
    first_doc = jnp.where(first_a < 0, first_b, first_a)
    last_doc = jnp.where(blank_b, last_a, last_b)
    return (memory, normer, stabil, log_a + log_b, first_doc, last_doc)


def local(
    queries,
    keys,
    values,
    output_gate_logits,
    input_gate_log,
    forget_gate_logits,
    extra_decay_log,
    document,
    residual,
    cell_norm_gain,
    output_weight,
    mixer_norm_gain,
    up_weight,
    down_weight,
):
    query_heads, final_state, output_rows = within_block_pass(
        queries, keys, values, input_gate_log, forget_gate_logits, extra_decay_log, document
    )
    numerator, denominator, peak_log, cumulative = output_rows
    memory, normer, stabil, last_doc = final_state
    step_logs = cumulative[:, :, -1]
    offsets = jnp.cumsum(step_logs, axis=0) - step_logs
    through = cumulative + offsets[:, :, None]
    summary = (memory, normer, stabil, jnp.sum(step_logs, axis=0), document[0], last_doc)
    identity = (
        jnp.zeros_like(memory),
        jnp.zeros_like(normer),
        jnp.full_like(stabil, NEG),
        jnp.zeros_like(stabil),
        jnp.array(-1, jnp.int32),
        jnp.array(-1, jnp.int32),
    )
    prefix = carried_in(summary, "sp", join_states, identity)
    doc_blocks = document.reshape(-1, BLOCK)
    carried_log = jnp.where(
        (doc_blocks == prefix[5])[:, None, :], through + prefix[2][None, :, None], NEG
    )
    merged_peak = jnp.maximum(peak_log, carried_log)
    own_weight = jnp.exp(peak_log - merged_peak)
    far_weight = jnp.exp(carried_log - merged_peak)
    numerator = own_weight[..., None] * numerator + far_weight[..., None] * jnp.einsum(
        "nhtd,hde->nhte", query_heads, prefix[0], precision=HIGH
    )
    denominator = own_weight * denominator + far_weight * jnp.einsum(
        "nhtd,hd->nht", query_heads, prefix[1], precision=HIGH
    )
    cell_out = numerator / jnp.maximum(jnp.abs(denominator), 1.0)[..., None]
    mixed = head_mix(cell_out, output_gate_logits, cell_norm_gain)
    head_terms = jnp.dot(mixed, output_weight, preferred_element_type=jnp.float32)
    width = residual.shape[1]
    model_width = width * lax.axis_size("tp")
    own_sum = lax.psum_scatter(
        head_terms.astype(jnp.bfloat16), "tp", scatter_dimension=1, tiled=True
    ).astype(jnp.float32)
    first_sum = (residual.astype(jnp.float32) + own_sum).astype(jnp.bfloat16)
    first_wide = lax.optimization_barrier(first_sum).astype(jnp.float32)
    squares = lax.psum(jnp.sum(first_wide * first_wide, axis=1), "tp")
    inverse = lax.rsqrt(squares / model_width + EPS)
    normed_own = (first_wide * inverse[:, None] * mixer_norm_gain.astype(jnp.float32)).astype(
        jnp.bfloat16
    )
    normed_full = lax.all_gather(normed_own, "tp", axis=1, tiled=True)
    hidden = jnp.dot(
        normed_full,
        lax.all_gather(up_weight, "sp", axis=0, tiled=True),
        preferred_element_type=jnp.float32,
    )
    squared = jnp.square(jax.nn.relu(hidden)).astype(jnp.bfloat16)
    channel = jnp.dot(
        squared,
        lax.all_gather(down_weight, "sp", axis=1, tiled=True),
        preferred_element_type=jnp.float32,
    )
    own_channel = lax.psum_scatter(
        channel.astype(jnp.bfloat16), "tp", scatter_dimension=1, tiled=True
    ).astype(jnp.float32)
    return (lax.optimization_barrier(first_sum).astype(jnp.float32) + own_channel).astype(
        jnp.bfloat16
    )


MESH = pl.DeviceIdType.MESH
F32 = jnp.float32
BF16 = jnp.bfloat16
CHUNKS = 2


def to_columns(rows):
    pad = jnp.zeros((128 - rows.shape[0], rows.shape[1]), F32)
    return jnp.transpose(jnp.concatenate([rows, pad], axis=0))


def to_rows(column):
    return jnp.transpose(jnp.broadcast_to(column, (column.shape[0], 128)))[0:8, :]


def halves(wide):
    high = wide.astype(BF16)
    return high, (wide - high.astype(F32)).astype(BF16)


def two_pass(wide, narrow):
    high, low = halves(wide)
    return jnp.dot(high, narrow, preferred_element_type=F32) + jnp.dot(
        low, narrow, preferred_element_type=F32
    )


def layer_kernel(
    n,
    m,
    back,
    q_ref,
    k_ref,
    v_ref,
    og_ref,
    forget_ref,
    extra_ref,
    input_ref,
    doc_ref,
    resid_ref,
    cell_gain_ref,
    mixer_gain_ref,
    wout_ref,
    up_ref,
    down_ref,
    out_ref,
    up_all,
    down_all,
    wcols,
    state_out,
    state_in,
    tail_out,
    tail_in,
    numer_ref,
    y_all,
    squares_out,
    squares_in,
    first_ref,
    normed,
    sums_out,
    sums_in,
    squared,
    parts,
    sib_in,
    comb,
    rs_in,
    w_send,
    w_recv,
    z_send,
    z_recv,
    y_send,
    y_recv,
    state_send,
    state_recv,
    tail_send,
    tail_recv,
    mix_send,
    mix_recv,
    squares_send,
    squares_recv,
    normed_send,
    normed_recv,
    sums_send,
    sums_recv,
    sib_send,
    sib_recv,
    rs_send,
    rs_recv,
):
    sp, tp = lax.axis_index("sp"), lax.axis_index("tp")
    rows, heads = q_ref.shape[0], q_ref.shape[1] // DH
    depth, hidden_width = up_ref.shape
    own_width = hidden_width // 2
    width = resid_ref.shape[1]
    up_piece, down_piece = depth // CHUNKS, own_width // CHUNKS
    z, y = sp // 2, sp % 2
    p, x, c = z % 2, tp // 2, tp % 2

    def z_at(j):
        return (z, z + 1 - 2 * p, z + 2 - 4 * (z // 2), n // 2 - 1 - z)[j]

    def tp_at(bits):
        far_c = c + (bits % 2) * (1 - 2 * c)
        far_x = x + ((bits // 2) % 2) * (1 - 2 * x)
        return 2 * far_x + far_c

    partner = 2 * z_at(1) + y
    beside = 2 * z + 1 - y

    barrier = pltpu.get_barrier_semaphore()
    for k in range(1, n):
        pl.semaphore_signal(barrier, device_id=((sp + k) % n, tp), device_id_type=MESH)
    for k in range(1, m):
        pl.semaphore_signal(barrier, device_id=(sp, (tp + k) % m), device_id_type=MESH)
    pl.semaphore_signal(barrier, device_id=(partner, tp_at(2)), device_id_type=MESH)
    pl.semaphore_wait(barrier, n + m - 1)

    def remote(src, dst, send_sem, recv_sem, device):
        return pltpu.make_async_remote_copy(
            src_ref=src,
            dst_ref=dst,
            send_sem=send_sem,
            recv_sem=recv_sem,
            device_id=device,
            device_id_type=MESH,
        )

    def cols_of(owner):
        return pl.ds(pl.multiple_of(owner * width, width), width)

    def w_copy(k):
        return remote(
            wout_ref.at[:, cols_of(tp_at(k))],
            wcols.at[tp],
            w_send.at[k - 1],
            w_recv.at[k - 1],
            (sp, tp_at(k)),
        )

    def w_arrival(k):
        there = wcols.at[tp_at(k)]
        return remote(there, there, w_send.at[k - 1], w_recv.at[k - 1], (sp, tp_at(k)))

    def slot(stream, block, piece):
        if stream == 0:
            start = pl.multiple_of(block * depth + piece * up_piece, up_piece)
            return up_all.at[pl.ds(start, up_piece), :]
        return down_all.at[block, pl.ds(piece * down_piece, down_piece), :]

    def own_piece(stream, half, piece):
        if stream == 0:
            lanes = pl.ds(pl.multiple_of(half * own_width, own_width), own_width)
            return up_ref.at[pl.ds(piece * up_piece, up_piece), lanes]
        deep = pl.multiple_of(half * own_width + piece * down_piece, down_piece)
        return down_ref.at[pl.ds(deep, down_piece), :]

    def z_copy(stream, j, piece):
        return remote(
            own_piece(stream, z_at(j) % 2, piece),
            slot(stream, sp, piece),
            z_send.at[stream, j - 1, piece],
            z_recv.at[stream, j - 1, piece],
            (2 * z_at(j) + y, tp),
        )

    def z_arrival(stream, j, piece):
        there = slot(stream, 2 * z_at(j) + y, piece)
        return remote(
            there,
            there,
            z_send.at[stream, j - 1, piece],
            z_recv.at[stream, j - 1, piece],
            (2 * z_at(j) + y, tp),
        )

    def y_copy(stream, i, piece):
        there = slot(stream, 2 * z_at(i) + y, piece)
        return remote(
            own_piece(stream, p, piece) if i == 0 else there,
            there,
            y_send.at[stream, i, piece],
            y_recv.at[stream, i, piece],
            (beside, tp),
        )

    def y_arrival(stream, i, piece):
        there = slot(stream, 2 * z_at(i) + 1 - y, piece)
        return remote(
            there,
            there,
            y_send.at[stream, i, piece],
            y_recv.at[stream, i, piece],
            (beside, tp),
        )

    events = [(0, j, piece) for piece in range(CHUNKS) for j in range(1, n // 2)]
    events += [(1, j, piece) for j in range(1, n // 2) for piece in range(CHUNKS)]
    done = [0]

    def pump(until):
        while done[0] < until:
            stream, j, piece = events[done[0]]
            done[0] += 1
            z_arrival(stream, j, piece).wait_recv()
            y_copy(stream, j, piece).start()

    ups = CHUNKS * (n // 2 - 1)

    for k in range(1, m):
        w_copy(k).start()
    for j in range(1, n // 2):
        z_copy(0, j, 0).start()
    y_copy(0, 0, 0).start()

    document = doc_ref[...].astype(F32)
    across = lax.broadcasted_iota(jnp.int32, (rows, rows), 1)
    along = lax.broadcasted_iota(jnp.int32, (rows, rows), 0)
    upper = (along <= across).astype(BF16)
    forget = jax.nn.log_sigmoid(forget_ref[...]) + extra_ref[...]
    high = forget.astype(BF16).astype(F32)
    middle = (forget - high).astype(BF16).astype(F32)
    low = forget - high - middle
    slab = lax.broadcasted_iota(jnp.int32, (8, rows), 0)
    split = jnp.zeros((8, rows), F32)
    for h in range(heads):
        for i, part in enumerate((high, middle, low)):
            split = jnp.where(slab == heads * i + h, part[h : h + 1, :], split)
    summed = jnp.dot(split.astype(BF16), upper, preferred_element_type=F32)
    last_doc = document[:, rows - 1 : rows]
    sums, entry, totals, stabs, scaled = [], [], [], [], []
    for h in range(heads):
        line_sum = summed[h : h + 1, :]
        for i in range(1, 3):
            line_sum = line_sum + summed[heads * i + h : heads * i + h + 1, :]
        sums.append(line_sum)
        entry.append(input_ref[h : h + 1, :] - line_sum)
        total = line_sum[:, rows - 1 : rows]
        keep = jnp.where(document == last_doc, total + entry[h], NEG)
        stab = jnp.max(keep, axis=1, keepdims=True)
        totals.append(total)
        stabs.append(stab)
        scaled.append(jnp.exp(keep - stab))
    packed = jnp.broadcast_to(document, (8, rows))
    for h in range(heads):
        packed = jnp.where(slab == h, sums[h], packed)
        packed = jnp.where(slab == heads + h, scaled[h], packed)
    columns = to_columns(packed)
    doc_col = columns[:, 2 * heads : 2 * heads + 1]
    line = lax.broadcasted_iota(jnp.int32, (8, DH), 0)
    for h in range(heads):
        mine = slice(h * DH, (h + 1) * DH)
        weighted = k_ref[:, mine].astype(F32) * columns[:, heads + h : heads + h + 1]
        state_out[h] = lax.dot_general(
            weighted.astype(BF16),
            v_ref[:, mine],
            (((0,), (0,)), ((), ())),
            preferred_element_type=F32,
        ).astype(BF16)
        tail = jnp.broadcast_to(jnp.sum(weighted, axis=0, keepdims=True), (8, DH))
        tail = jnp.where(line == 1, stabs[h], tail)
        tail = jnp.where(line == 2, totals[h], tail)
        tail = jnp.where(line == 3, last_doc, tail)
        tail_out[h] = tail

    def state_copies(k):
        return [
            remote(src, dst.at[k - 1], send_sem.at[k - 1], recv_sem.at[k - 1], ((sp + k) % n, tp))
            for src, dst, send_sem, recv_sem in (
                (tail_out, tail_in, tail_send, tail_recv),
                (state_out, state_in, state_send, state_recv),
            )
        ]

    for k in range(1, back + 1):

        @pl.when(sp + k < n)
        def _():
            for copy in state_copies(k):
                copy.start()

        @pl.when(sp < k)
        def _():
            tail_in[k - 1] = jnp.zeros((heads, 8, DH), F32)
            state_in[k - 1] = jnp.zeros((heads, DH, DH), BF16)

    for piece in range(1, CHUNKS):
        for j in range(1, n // 2):
            z_copy(0, j, piece).start()
        y_copy(0, 0, piece).start()

    half_lanes = pl.ds(pl.multiple_of(p * own_width, own_width), own_width)
    up_all[pl.ds(pl.multiple_of(sp * depth, depth), depth), :] = up_ref[:, half_lanes]
    down_all[sp] = down_ref[half_lanes, :]

    step = min(rows, 256)
    locals_of = []
    for h in range(heads):
        mine = slice(h * DH, (h + 1) * DH)
        peaks, denoms = [], []
        for start in range(0, rows, step):
            stop = start + step
            here = slice(start, stop)
            scores = lax.dot_general(
                q_ref[here, mine],
                k_ref[0:stop, mine],
                (((1,), (1,)), ((), ())),
                preferred_element_type=F32,
            ) * (DH**-0.5)
            pair = columns[here, h : h + 1] + entry[h][:, 0:stop]
            seen = (doc_col[here] == document[:, 0:stop]) & (
                along[here, 0:stop] >= across[here, 0:stop]
            )
            pair = jnp.where(seen, pair, NEG)
            peak = jnp.max(pair, axis=1, keepdims=True)
            scores = scores * jnp.exp(pair - peak)
            numer_ref[h, here, :] = two_pass(scores, v_ref[0:stop, mine])
            peaks.append(peak)
            denoms.append(jnp.sum(scores, axis=1, keepdims=True))
        locals_of.append((jnp.concatenate(peaks, axis=0), jnp.concatenate(denoms, axis=0)))
        pump(PUMPS_LOCAL[h] if h < len(PUMPS_LOCAL) else 0)

    for k in range(1, back + 1):

        @pl.when(sp >= k)
        def _():
            for copy in state_copies(k):
                copy.wait_recv()

    def mix_copy(k, h):
        here = y_all.at[tp, :, pl.ds(h * DH, DH)]
        return remote(
            here, here, mix_send.at[k - 1, h], mix_recv.at[k - 1, h], (sp, tp_at(k))
        )

    def mix_forward(h):
        there = y_all.at[tp_at(2), :, pl.ds(h * DH, DH)]
        return remote(there, there, mix_send.at[2, h], mix_recv.at[2, h], (sp, tp_at(1)))

    def mix_arrival(k, h):
        there = y_all.at[tp_at(k), :, pl.ds(h * DH, DH)]
        return remote(
            there, there, mix_send.at[k - 1, h], mix_recv.at[k - 1, h], (sp, tp_at(k))
        )

    first_doc = document[:, 0:1]
    square_sum = jnp.zeros((rows, DH), F32)
    for h in range(heads):
        mine = slice(h * DH, (h + 1) * DH)
        between = jnp.zeros((1, DH), F32)
        logs, valids = [], []
        best = jnp.full((1, DH), NEG, F32)
        for k in range(1, back + 1):
            tail = tail_in[k - 1, h]
            far = lax.broadcasted_iota(jnp.int32, (1, DH), 1) * 0 + sp
            valid = (tail[3:4, :] == first_doc) & (far >= k)
            log = jnp.where(valid, between + tail[1:2, :], NEG)
            between = between + tail[2:3, :]
            best = jnp.maximum(best, log)
            logs.append(log)
            valids.append(valid)
        memory = jnp.zeros((DH, DH), F32)
        normer = jnp.zeros((1, DH), F32)
        for k in range(1, back + 1):
            weight = jnp.where(valids[k - 1], jnp.exp(logs[k - 1] - best), 0.0)
            memory = memory + jnp.where(
                valids[k - 1], weight * state_in[k - 1, h].astype(F32), 0.0
            )
            normer = normer + jnp.where(
                valids[k - 1], weight * tail_in[k - 1, h, 0:1, :], 0.0
            )
        peak, denom = locals_of[h]
        carried = jnp.where(doc_col == first_doc, columns[:, h : h + 1] + best[:, 0:1], NEG)
        merged = jnp.maximum(peak, carried)
        own = jnp.exp(peak - merged)
        other = jnp.exp(carried - merged) * (DH**-0.5)
        query = q_ref[:, mine]
        high, low = halves(memory)
        reached = jnp.dot(query, high, preferred_element_type=F32) + jnp.dot(
            query, low, preferred_element_type=F32
        )
        numer = own * numer_ref[h] + other * reached
        denom = own * denom + other * jnp.sum(
            query.astype(F32) * normer, axis=1, keepdims=True
        )
        cell = numer / jnp.maximum(jnp.abs(denom), 1.0)
        square_sum = square_sum + cell * cell
        gated = jax.nn.sigmoid(og_ref[:, mine].astype(F32))
        y_all[tp, :, mine] = (gated * cell * cell_gain_ref[:, mine].astype(F32)).astype(BF16)
        for k in range(1, 3):
            mix_copy(k, h).start()
    squares_out[...] = to_rows(jnp.sum(square_sum, axis=1, keepdims=True))

    def square_copy(k):
        return remote(
            squares_out,
            squares_in.at[k - 1],
            squares_send.at[k - 1],
            squares_recv.at[k - 1],
            (sp, tp_at(k)),
        )

    for k in range(1, m):
        square_copy(k).start()
    here = cols_of(tp)
    attn = jnp.dot(y_all[tp], wout_ref[:, here], preferred_element_type=F32)
    pump(PUMPS_MIX)
    for h in range(heads):
        mix_arrival(2, h).wait_recv()
        mix_forward(h).start()
    for k in (1, 2, 3):
        w_arrival(k).wait_recv()
        if k != 2:
            for h in range(heads):
                mix_arrival(k, h).wait_recv()
        attn = attn + jnp.dot(
            y_all[tp_at(k)], wcols[tp_at(k)], preferred_element_type=F32
        )
    squares = squares_out[...]
    for k in range(1, m):
        square_copy(k).wait_recv()
        squares = squares + squares_in[k - 1]
    inverse = lax.rsqrt(to_columns(squares)[:, 0:1] / (heads * DH * m) + EPS)
    first = (resid_ref[...].astype(F32) + attn * inverse).astype(BF16)
    first_ref[...] = first
    first = first.astype(F32)

    def plane(bit):
        return p + bit * (1 - 2 * p)

    def rows_of(bit):
        return pl.ds(pl.multiple_of(plane(bit) * rows, rows), rows)

    normed[rows_of(0), here] = (first * mixer_gain_ref[...].astype(F32)).astype(BF16)

    def group_at(bits):
        return (sp + (bits // 4) * (partner - sp), tp_at(bits % 4))

    def normed_block(bits):
        return normed.at[rows_of(bits // 4), cols_of(tp_at(bits % 4))]

    def normed_copy(source, flip):
        block = normed_block(source)
        rel = source + flip - 1
        return remote(block, block, normed_send.at[rel], normed_recv.at[rel], group_at(flip))

    def normed_arrival(rel):
        block = normed_block(rel)
        return remote(
            block, block, normed_send.at[rel - 1], normed_recv.at[rel - 1], group_at(rel % 2 or rel)
        )

    routes = ((0, 2), (0, 4), (0, 1), (2, 1), (4, 2), (4, 1), (6, 1))
    for route in routes[:3]:
        normed_copy(*route).start()
    sums_out[0] = to_rows(jnp.sum(first * first, axis=1, keepdims=True))

    def sums_copy(k):
        return remote(
            sums_out.at[k // 4],
            sums_in.at[k - 1],
            sums_send.at[k - 1],
            sums_recv.at[k - 1],
            group_at(k),
        )

    for k in range(1, m):
        sums_copy(k).start()

    for j in range(1, n // 2):
        for piece in range(CHUNKS):
            z_copy(1, j, piece).start()
    for piece in range(CHUNKS):
        y_copy(1, 0, piece).start()

    total = sums_out[0]
    for k in range(1, m):
        sums_copy(k).wait_recv()
        total = total + sums_in[k - 1]
    sums_out[1] = total
    sums_copy(4).start()

    normed_arrival(2).wait_recv()
    normed_copy(2, 1).start()
    pump(PUMPS_NORMED)
    normed_arrival(4).wait_recv()
    normed_copy(4, 2).start()
    normed_copy(4, 1).start()
    normed_arrival(1).wait_recv()
    normed_arrival(3).wait_recv()
    pump(ups)
    for i in range(n // 2):
        for piece in range(CHUNKS):
            y_arrival(0, i, piece).wait_recv()

    tile = min(own_width, 256)

    def up_half(bit, line_sums):
        scale = lax.rsqrt(to_columns(line_sums)[:, 0:1] / (width * m) + EPS)

        def up_tile(t, carry):
            cols = pl.ds(pl.multiple_of(t * tile, tile), tile)
            raw = jnp.dot(normed[rows_of(bit), :], up_all[:, cols], preferred_element_type=F32)
            hidden = jnp.maximum(raw * scale, 0.0)
            squared[rows_of(bit), cols] = (hidden * hidden).astype(BF16)
            return carry

        lax.fori_loop(0, own_width // tile, up_tile, 0)

    up_half(0, total)
    normed_arrival(6).wait_recv()
    normed_copy(6, 1).start()
    normed_arrival(5).wait_recv()
    normed_arrival(7).wait_recv()
    sums_copy(4).wait_recv()
    up_half(1, sums_in[3])

    blocks = [(j, side) for j in range(n // 2) for side in range(2)]

    def place(i):
        j, side = blocks[i]
        owner = z_at(j)
        return owner, owner // 2, y + side * (1 - 2 * y)

    def sib_copy(i):
        _, far_x, half = place(i)
        return remote(
            parts.at[i],
            sib_in.at[far_x, half],
            sib_send.at[far_x, half],
            sib_recv.at[far_x, half],
            (sp, tp_at(1)),
        )

    def rs_copy(i, cross):
        _, far_x, half = place(i)
        turn = (far_x + x) % 2
        rel = turn + 2 * cross - 1
        return turn, remote(
            comb.at[far_x, half, rows_of(cross), :],
            rs_in.at[rel, half],
            rs_send.at[far_x, half, cross],
            rs_recv.at[rel, half],
            (sp + cross * (partner - sp), 2 * far_x + c),
        )

    def down_block(i):
        j, side = blocks[i]
        owner, _, half = place(i)
        block = 2 * owner + half
        for bit in range(2):
            there = slice(bit * rows, (bit + 1) * rows)
            parts[i, there, :] = jnp.dot(
                squared[there, :], down_all[block], preferred_element_type=F32
            ).astype(BF16)

        @pl.when(owner % 2 != c)
        def _():
            sib_copy(i).start()

    def combine(i):
        owner, far_x, half = place(i)

        @pl.when(owner % 2 == c)
        def _():
            sib_copy(i).wait_recv()
            comb[far_x, half] = (
                parts[i].astype(F32) + sib_in[far_x, half].astype(F32)
            ).astype(BF16)
            rs_copy(i, 1)[1].start()
            turn, copy = rs_copy(i, 0)

            @pl.when(turn == 1)
            def _():
                copy.start()

    for i, (j, side) in enumerate(blocks):
        if side == 0:
            if j > 0:
                pump(ups + CHUNKS * j)
        else:
            for piece in range(CHUNKS):
                y_arrival(1, j, piece).wait_recv()
        down_block(i)
        if i > 0:
            combine(i - 1)
    combine(len(blocks) - 1)

    for half in range(2):
        cols = slice(half * depth, (half + 1) * depth)
        total = first_ref[:, cols].astype(F32) + comb[x, half, rows_of(0), :].astype(F32)
        for rel in range(1, 4):
            there = rs_in.at[rel - 1, half]
            remote(
                there,
                there,
                rs_send.at[0, 0, 0],
                rs_recv.at[rel - 1, half],
                group_at(2 * (rel % 2) + 4 * (rel // 2)),
            ).wait_recv()
            total = total + rs_in[rel - 1, half].astype(F32)
        out_ref[:, cols] = total.astype(BF16)

    for k in range(1, m):
        w_copy(k).wait_send()
        square_copy(k).wait_send()
        for h in range(heads):
            (mix_copy(k, h) if k < 3 else mix_forward(h)).wait_send()
    for k in range(1, m + 1):
        sums_copy(k).wait_send()
    for route in routes:
        normed_copy(*route).wait_send()
    for stream in range(2):
        for piece in range(CHUNKS):
            for j in range(1, n // 2):
                z_copy(stream, j, piece).wait_send()
            for i in range(n // 2):
                y_copy(stream, i, piece).wait_send()
    for k in range(1, back + 1):

        @pl.when(sp + k < n)
        def _():
            for copy in state_copies(k):
                copy.wait_send()

    for i in range(len(blocks)):
        owner = place(i)[0]

        @pl.when(owner % 2 != c)
        def _():
            sib_copy(i).wait_send()

        @pl.when(owner % 2 == c)
        def _():
            rs_copy(i, 1)[1].wait_send()
            turn, copy = rs_copy(i, 0)

            @pl.when(turn == 1)
            def _():
                copy.wait_send()


PUMPS_LOCAL = (0, 1)
PUMPS_MIX = 2
PUMPS_NORMED = 5


def fused(
    n,
    m,
    queries,
    keys,
    values,
    output_gate_logits,
    input_gate_log,
    forget_gate_logits,
    extra_decay_log,
    document,
    residual,
    cell_norm_gain,
    output_weight,
    mixer_norm_gain,
    up_weight,
    down_weight,
):
    rows, heads = queries.shape[0], queries.shape[1] // DH
    depth, hidden_width = up_weight.shape
    width = residual.shape[1]
    own_width = hidden_width // 2
    back = min(n - 1, (MOST - 2) // rows + 1)
    dma = pltpu.SemaphoreType.DMA
    lines = n // 2
    return pl.pallas_call(
        functools.partial(layer_kernel, n, m, back),
        out_shape=jax.ShapeDtypeStruct((rows, width), BF16),
        in_specs=[pl.BlockSpec(memory_space=pltpu.VMEM)] * 14,
        out_specs=pl.BlockSpec(memory_space=pltpu.VMEM),
        scratch_shapes=[
            pltpu.VMEM((n * depth, own_width), BF16),
            pltpu.VMEM((n, own_width, depth), BF16),
            pltpu.VMEM((m, heads * DH, width), BF16),
            pltpu.VMEM((heads, DH, DH), BF16),
            pltpu.VMEM((back, heads, DH, DH), BF16),
            pltpu.VMEM((heads, 8, DH), F32),
            pltpu.VMEM((back, heads, 8, DH), F32),
            pltpu.VMEM((heads, rows, DH), F32),
            pltpu.VMEM((m, rows, heads * DH), BF16),
            pltpu.VMEM((8, rows), F32),
            pltpu.VMEM((m - 1, 8, rows), F32),
            pltpu.VMEM((rows, width), BF16),
            pltpu.VMEM((2 * rows, m * width), BF16),
            pltpu.VMEM((2, 8, rows), F32),
            pltpu.VMEM((m, 8, rows), F32),
            pltpu.VMEM((2 * rows, own_width), BF16),
            pltpu.VMEM((n, 2 * rows, depth), BF16),
            pltpu.VMEM((2, 2, 2 * rows, depth), BF16),
            pltpu.VMEM((2, 2, 2 * rows, depth), BF16),
            pltpu.VMEM((3, 2, rows, depth), BF16),
            dma((m - 1,)),
            dma((m - 1,)),
            dma((2, lines - 1, CHUNKS)),
            dma((2, lines - 1, CHUNKS)),
            dma((2, lines, CHUNKS)),
            dma((2, lines, CHUNKS)),
            dma((back,)),
            dma((back,)),
            dma((back,)),
            dma((back,)),
            dma((m - 1, heads)),
            dma((m - 1, heads)),
            dma((m - 1,)),
            dma((m - 1,)),
            dma((2 * m - 1,)),
            dma((2 * m - 1,)),
            dma((m,)),
            dma((m,)),
            dma((2, 2)),
            dma((2, 2)),
            dma((2, 2, 2)),
            dma((3, 2)),
        ],
        compiler_params=pltpu.CompilerParams(
            collective_id=0, has_side_effects=True, vmem_limit_bytes=60 * 1024 * 1024
        ),
        name="layer",
    )(
        queries,
        keys,
        values,
        output_gate_logits,
        forget_gate_logits.T,
        extra_decay_log.T,
        input_gate_log.T,
        document[None, :],
        residual,
        cell_norm_gain[None, :],
        mixer_norm_gain[None, :],
        output_weight,
        up_weight,
        down_weight,
    )


def either(n, m, *args):
    depth, hidden_width = args[12].shape
    heads = args[0].shape[1] // DH
    fits = n == 8 and m == 4 and depth % 128 == 0 and hidden_width % 512 == 0
    fits = fits and 3 * heads <= 8 and args[8].shape[1] == 2 * depth
    fits = fits and args[0].shape[0] % 256 == 0
    if fits:
        return fused(n, m, *args)
    return local(*args)


def solution(mesh):
    in_specs = (
        P("sp", "tp"),
        P("sp", "tp"),
        P("sp", "tp"),
        P("sp", "tp"),
        P("sp", "tp"),
        P("sp", "tp"),
        P("sp", "tp"),
        P("sp"),
        P("sp", "tp"),
        P("tp"),
        P("tp", None),
        P("tp"),
        P("sp", "tp"),
        P("tp", "sp"),
    )
    out_specs = P("sp", "tp")
    body = functools.partial(either, mesh.shape["sp"], mesh.shape["tp"])
    return jax.shard_map(body, mesh=mesh, in_specs=in_specs, out_specs=out_specs, check_vma=False)
```

time: 187 us -> 167 us (0.89)
  the two profiles are of different devices: /device:TPU:23 before, /device:TPU:24 now
where the time goes in v1:
time: 167 us; the launch traced here: 166 us
  Pallas kernels  162 us (97%)
  local copies, waits for them, and re-layouts  3.78 us (2%)
    pallas_call x1, Pallas kernels, fused(): pl.pallas_call(functools.partial(layer_kernel, n, m, back), out_shape=jax...  162 us

profile of v1, /device:TPU:24, one launch (start us, length us, event | category | flops | bytes accessed | tf_op | source)
XLA Modules:
  0.0 165.8 jit_solution(3735085166103890687)
XLA Ops:
  0.0 0.0 copy-start.1
  0.0 0.7 copy-done.1
  0.7 0.0 copy-start
  0.7 0.6 broadcast_in_dim.10.cell_gain_ref
  1.2 0.1 copy-done
  1.3 0.6 broadcast_in_dim.11.mixer_gain_ref
  1.9 162.0 %layer.1 = bf16[512,512]{1,0:T(8,128)(2,1)} custom-call(bf16[512,256]{1,0:T(8,128)(2,1)} %q_ref.1, bf16[512,256]{1,0:T(8,128)(2,1)} %k_ref.1, bf16[512,256]{1,0:T(8,128)(2,1)} %v_ref.1, bf16[512,256]{1,0:T(8,128)(2,1)} %og_ref.1, f32[2,512]{1,0:T(2,128)} %bitcast.4, f32[2,512]{1,0:T(2,128)} %bitcast.5, f32[2,512]{1,0:T(2,128)} %bitcast.6, s32[1,512]{1,0:T(1,128)} %bitcast.7, ...), custom_call_target="tpu_custom_call" | custom-call | tf_op jit(solution)/shard_map/layer/pallas_call | solution.py:885
  163.9 1.9 %copy.16 = bf16[512,512]{1,0:T(8,128)(2,1)} copy(bf16[512,512]{1,0:T(8,128)(2,1)} %layer.1) | data formatting | bytes 1048576
Async XLA Ops:
  0.0 0.7 copy-start.1
  0.7 0.7 copy-start

commit v2 on v1

--- a/solution.py
+++ b/solution.py
@@ -261,8 +261,12 @@
     down_all,
     wcols,
     state_out,
+    near_state,
+    pair_state,
     state_in,
     tail_out,
+    near_tail,
+    pair_tail,
     tail_in,
     numer_ref,
     y_all,
@@ -276,17 +280,20 @@
     parts,
     sib_in,
     comb,
-    rs_in,
+    x_in,
+    last_out,
+    last_in,
     w_send,
     w_recv,
     z_send,
     z_recv,
+    relay_send,
     y_send,
     y_recv,
+    near_send,
+    near_recv,
     state_send,
     state_recv,
-    tail_send,
-    tail_recv,
     mix_send,
     mix_recv,
     squares_send,
@@ -297,16 +304,18 @@
     sums_recv,
     sib_send,
     sib_recv,
-    rs_send,
-    rs_recv,
+    x_send,
+    x_recv,
+    last_send,
+    last_recv,
 ):
     sp, tp = lax.axis_index("sp"), lax.axis_index("tp")
     rows, heads = q_ref.shape[0], q_ref.shape[1] // DH
     depth, hidden_width = up_ref.shape
     own_width = hidden_width // 2
     width = resid_ref.shape[1]
-    up_piece, down_piece = depth // CHUNKS, own_width // CHUNKS
-    z, y = sp // 2, sp % 2
+    up_piece, down_piece = depth // CHUNKS, depth // CHUNKS
+    z, y, lines = sp // 2, sp % 2, n // 2
     p, x, c = z % 2, tp // 2, tp % 2
 
     def z_at(j):
@@ -325,8 +334,7 @@
         pl.semaphore_signal(barrier, device_id=((sp + k) % n, tp), device_id_type=MESH)
     for k in range(1, m):
         pl.semaphore_signal(barrier, device_id=(sp, (tp + k) % m), device_id_type=MESH)
-    pl.semaphore_signal(barrier, device_id=(partner, tp_at(2)), device_id_type=MESH)
-    pl.semaphore_wait(barrier, n + m - 1)
+    pl.semaphore_wait(barrier, n + m - 2)
 
     def remote(src, dst, send_sem, recv_sem, device):
         return pltpu.make_async_remote_copy(
@@ -358,14 +366,14 @@
         if stream == 0:
             start = pl.multiple_of(block * depth + piece * up_piece, up_piece)
             return up_all.at[pl.ds(start, up_piece), :]
-        return down_all.at[block, pl.ds(piece * down_piece, down_piece), :]
+        return down_all.at[block, piece]
 
     def own_piece(stream, half, piece):
         if stream == 0:
             lanes = pl.ds(pl.multiple_of(half * own_width, own_width), own_width)
             return up_ref.at[pl.ds(piece * up_piece, up_piece), lanes]
-        deep = pl.multiple_of(half * own_width + piece * down_piece, down_piece)
-        return down_ref.at[pl.ds(deep, down_piece), :]
+        deep = pl.ds(pl.multiple_of(half * own_width, own_width), own_width)
+        return down_ref.at[deep, pl.ds(piece * down_piece, down_piece)]
 
     def z_copy(stream, j, piece):
         return remote(
@@ -376,6 +384,18 @@
             (2 * z_at(j) + y, tp),
         )
 
+    inner = p + z // 2 == 1
+
+    def z_forward(stream, piece):
+        there = slot(stream, 2 * z_at(1) + y, piece)
+        return remote(
+            there,
+            there,
+            relay_send.at[stream, piece],
+            z_recv.at[stream, 2, piece],
+            (2 * z_at(2) + y, tp),
+        )
+
     def z_arrival(stream, j, piece):
         there = slot(stream, 2 * z_at(j) + y, piece)
         return remote(
@@ -406,24 +426,27 @@
             (beside, tp),
         )
 
-    events = [(0, j, piece) for piece in range(CHUNKS) for j in range(1, n // 2)]
-    events += [(1, j, piece) for j in range(1, n // 2) for piece in range(CHUNKS)]
+    order = ((1, 0), (1, 1), (2, 0), (3, 0), (2, 1), (3, 1))
+    events = [(stream, j, piece) for stream in range(2) for j, piece in order]
     done = [0]
 
     def pump(until):
         while done[0] < until:
-            stream, j, piece = events[done[0]]
+            event = done[0]
+            stream, j, piece = events[event]
             done[0] += 1
             z_arrival(stream, j, piece).wait_recv()
             y_copy(stream, j, piece).start()
-
-    ups = CHUNKS * (n // 2 - 1)
+            if j == 1:
+
+                @pl.when(inner)
+                def _():
+                    z_forward(stream, piece).start()
+
+    ups = len(order)
 
     for k in range(1, m):
         w_copy(k).start()
-    for j in range(1, n // 2):
-        z_copy(0, j, 0).start()
-    y_copy(0, 0, 0).start()
 
     document = doc_ref[...].astype(F32)
     across = lax.broadcasted_iota(jnp.int32, (rows, rows), 1)
@@ -475,35 +498,45 @@
         tail = jnp.where(line == 3, last_doc, tail)
         tail_out[h] = tail
 
+    def pair_of(refs, send_sem, recv_sem, device):
+        return [
+            remote(src, dst, send_sem.at[i], recv_sem.at[i], device)
+            for i, (src, dst) in enumerate(refs)
+        ]
+
+    def near_copies():
+        refs = ((tail_out, near_tail), (state_out, near_state))
+        return pair_of(refs, near_send, near_recv, (beside, tp))
+
     def state_copies(k):
-        return [
-            remote(src, dst.at[k - 1], send_sem.at[k - 1], recv_sem.at[k - 1], ((sp + k) % n, tp))
-            for src, dst, send_sem, recv_sem in (
-                (tail_out, tail_in, tail_send, tail_recv),
-                (state_out, state_in, state_send, state_recv),
-            )
-        ]
+        refs = ((pair_tail, tail_in.at[k - 1]), (pair_state, state_in.at[k - 1]))
+        return pair_of(
+            refs, state_send.at[k - 1], state_recv.at[k - 1], (2 * ((z + k) % lines) + y, tp)
+        )
+
+    for copy in near_copies():
+        copy.start()
+    z_copy(0, 1, 0).start()
+
+    @pl.when(inner)
+    def _():
+        z_copy(0, 3, 0).start()
+
+    for piece in range(CHUNKS):
+        y_copy(0, 0, piece).start()
 
     for k in range(1, back + 1):
 
-        @pl.when(sp + k < n)
-        def _():
-            for copy in state_copies(k):
-                copy.start()
-
-        @pl.when(sp < k)
+        @pl.when(z < k)
         def _():
             tail_in[k - 1] = jnp.zeros((heads, 8, DH), F32)
             state_in[k - 1] = jnp.zeros((heads, DH, DH), BF16)
 
-    for piece in range(1, CHUNKS):
-        for j in range(1, n // 2):
-            z_copy(0, j, piece).start()
-        y_copy(0, 0, piece).start()
-
     half_lanes = pl.ds(pl.multiple_of(p * own_width, own_width), own_width)
     up_all[pl.ds(pl.multiple_of(sp * depth, depth), depth), :] = up_ref[:, half_lanes]
-    down_all[sp] = down_ref[half_lanes, :]
+    for piece in range(CHUNKS):
+        cols = slice(piece * down_piece, (piece + 1) * down_piece)
+        down_all[sp, piece] = down_ref[half_lanes, cols]
 
     step = min(rows, 256)
     locals_of = []
@@ -530,11 +563,41 @@
             peaks.append(peak)
             denoms.append(jnp.sum(scores, axis=1, keepdims=True))
         locals_of.append((jnp.concatenate(peaks, axis=0), jnp.concatenate(denoms, axis=0)))
-        pump(PUMPS_LOCAL[h] if h < len(PUMPS_LOCAL) else 0)
+
+    for copy in near_copies():
+        copy.wait_recv()
+    for h in range(heads):
+        own_tail, far_tail = tail_out[h], near_tail[h]
+        old_tail = jnp.where(y == 0, own_tail, far_tail)
+        new_tail = jnp.where(y == 0, far_tail, own_tail)
+        own_state, far_state = state_out[h].astype(F32), near_state[h].astype(F32)
+        old_state = jnp.where(y == 0, own_state, far_state)
+        new_state = jnp.where(y == 0, far_state, own_state)
+        joined = old_tail[3:4, :] == new_tail[3:4, :]
+        old_log = jnp.where(joined, old_tail[1:2, :] + new_tail[2:3, :], NEG)
+        stab = jnp.maximum(old_log, new_tail[1:2, :])
+        old_weight = jnp.where(joined, jnp.exp(old_log - stab), 0.0)
+        new_weight = jnp.exp(new_tail[1:2, :] - stab)
+        pair_state[h] = (
+            jnp.where(joined, old_weight * old_state, 0.0) + new_weight * new_state
+        ).astype(BF16)
+        tail = jnp.where(joined, old_weight * old_tail, 0.0) + new_weight * new_tail
+        tail = jnp.where(line == 1, stab, tail)
+        tail = jnp.where(line == 2, old_tail + new_tail, tail)
+        pair_tail[h] = jnp.where(line == 3, new_tail, tail)
 
     for k in range(1, back + 1):
 
-        @pl.when(sp >= k)
+        @pl.when(z + k < lines)
+        def _():
+            for copy in state_copies(k):
+                copy.start()
+
+    z_copy(0, 1, 1).start()
+    z_copy(0, 2, 0).start()
+    for k in range(1, back + 1):
+
+        @pl.when(z >= k)
         def _():
             for copy in state_copies(k):
                 copy.wait_recv()
@@ -559,28 +622,25 @@
     square_sum = jnp.zeros((rows, DH), F32)
     for h in range(heads):
         mine = slice(h * DH, (h + 1) * DH)
+        earlier = [(near_tail, near_state, y == 1)]
+        earlier += [(tail_in.at[k], state_in.at[k], z > k) for k in range(back)]
         between = jnp.zeros((1, DH), F32)
         logs, valids = [], []
         best = jnp.full((1, DH), NEG, F32)
-        for k in range(1, back + 1):
-            tail = tail_in[k - 1, h]
-            far = lax.broadcasted_iota(jnp.int32, (1, DH), 1) * 0 + sp
-            valid = (tail[3:4, :] == first_doc) & (far >= k)
+        for tails, _, exists in earlier:
+            tail = tails[h]
+            valid = (tail[3:4, :] == first_doc) & jnp.broadcast_to(exists, (1, DH))
             log = jnp.where(valid, between + tail[1:2, :], NEG)
-            between = between + tail[2:3, :]
+            between = between + jnp.where(exists, tail[2:3, :], 0.0)
             best = jnp.maximum(best, log)
             logs.append(log)
             valids.append(valid)
         memory = jnp.zeros((DH, DH), F32)
         normer = jnp.zeros((1, DH), F32)
-        for k in range(1, back + 1):
-            weight = jnp.where(valids[k - 1], jnp.exp(logs[k - 1] - best), 0.0)
-            memory = memory + jnp.where(
-                valids[k - 1], weight * state_in[k - 1, h].astype(F32), 0.0
-            )
-            normer = normer + jnp.where(
-                valids[k - 1], weight * tail_in[k - 1, h, 0:1, :], 0.0
-            )
+        for i, (tails, states, _) in enumerate(earlier):
+            weight = jnp.where(valids[i], jnp.exp(logs[i] - best), 0.0)
+            memory = memory + jnp.where(valids[i], weight * states[h].astype(F32), 0.0)
+            normer = normer + jnp.where(valids[i], weight * tails[h, 0:1, :], 0.0)
         peak, denom = locals_of[h]
         carried = jnp.where(doc_col == first_doc, columns[:, h : h + 1] + best[:, 0:1], NEG)
         merged = jnp.maximum(peak, carried)
@@ -616,10 +676,17 @@
         square_copy(k).start()
     here = cols_of(tp)
     attn = jnp.dot(y_all[tp], wout_ref[:, here], preferred_element_type=F32)
-    pump(PUMPS_MIX)
+    pump(PUMPS[0])
+
+    @pl.when(inner)
+    def _():
+        for j in (2, 3):
+            z_copy(0, j, 1).start()
+
     for h in range(heads):
         mix_arrival(2, h).wait_recv()
         mix_forward(h).start()
+    pump(PUMPS[1])
     for k in (1, 2, 3):
         w_arrival(k).wait_recv()
         if k != 2:
@@ -663,8 +730,6 @@
         )
 
     routes = ((0, 2), (0, 4), (0, 1), (2, 1), (4, 2), (4, 1), (6, 1))
-    for route in routes[:3]:
-        normed_copy(*route).start()
     sums_out[0] = to_rows(jnp.sum(first * first, axis=1, keepdims=True))
 
     def sums_copy(k):
@@ -678,13 +743,8 @@
 
     for k in range(1, m):
         sums_copy(k).start()
-
-    for j in range(1, n // 2):
-        for piece in range(CHUNKS):
-            z_copy(1, j, piece).start()
-    for piece in range(CHUNKS):
-        y_copy(1, 0, piece).start()
-
+    for route in routes[:3]:
+        normed_copy(*route).start()
     total = sums_out[0]
     for k in range(1, m):
         sums_copy(k).wait_recv()
@@ -692,15 +752,41 @@
     sums_out[1] = total
     sums_copy(4).start()
 
+    @pl.when(jnp.logical_not(inner))
+    def _():
+        z_copy(0, 2, 1).start()
+
+    y_copy(1, 0, 0).start()
+    pump(PUMPS[2])
+    y_copy(1, 0, 1).start()
     normed_arrival(2).wait_recv()
     normed_copy(2, 1).start()
-    pump(PUMPS_NORMED)
     normed_arrival(4).wait_recv()
     normed_copy(4, 2).start()
     normed_copy(4, 1).start()
     normed_arrival(1).wait_recv()
     normed_arrival(3).wait_recv()
+    pump(ups - 1)
+
+    @pl.when(inner)
+    def _():
+        for j in (2, 3):
+            z_copy(1, j, 0).start()
+
     pump(ups)
+
+    z_copy(1, 1, 0).start()
+
+    @pl.when(jnp.logical_not(inner))
+    def _():
+        z_copy(1, 2, 0).start()
+
+    z_copy(1, 1, 1).start()
+
+    @pl.when(jnp.logical_not(inner))
+    def _():
+        z_copy(1, 2, 1).start()
+
     for i in range(n // 2):
         for piece in range(CHUNKS):
             y_arrival(0, i, piece).wait_recv()
@@ -720,50 +806,66 @@
         lax.fori_loop(0, own_width // tile, up_tile, 0)
 
     up_half(0, total)
+    pump(ups + 1)
+
+    @pl.when(inner)
+    def _():
+        for j in (2, 3):
+            z_copy(1, j, 1).start()
+
     normed_arrival(6).wait_recv()
     normed_copy(6, 1).start()
     normed_arrival(5).wait_recv()
     normed_arrival(7).wait_recv()
     sums_copy(4).wait_recv()
     up_half(1, sums_in[3])
-
-    blocks = [(j, side) for j in range(n // 2) for side in range(2)]
+    pump(ups + PUMPS[3])
+
+    pairs = [(0, piece) for piece in range(CHUNKS)] + list(order)
+    units = [(j, side, piece) for j, piece in pairs for side in range(2)]
 
     def place(i):
-        j, side = blocks[i]
+        j, side, piece = units[i]
         owner = z_at(j)
-        return owner, owner // 2, y + side * (1 - 2 * y)
+        return owner, owner // 2, y + side * (1 - 2 * y), piece
 
     def sib_copy(i):
-        _, far_x, half = place(i)
+        _, far_x, half, piece = place(i)
         return remote(
             parts.at[i],
-            sib_in.at[far_x, half],
-            sib_send.at[far_x, half],
-            sib_recv.at[far_x, half],
+            sib_in.at[far_x, half, piece],
+            sib_send.at[far_x, half, piece],
+            sib_recv.at[far_x, half, piece],
             (sp, tp_at(1)),
         )
 
-    def rs_copy(i, cross):
-        _, far_x, half = place(i)
-        turn = (far_x + x) % 2
-        rel = turn + 2 * cross - 1
-        return turn, remote(
-            comb.at[far_x, half, rows_of(cross), :],
-            rs_in.at[rel, half],
-            rs_send.at[far_x, half, cross],
-            rs_recv.at[rel, half],
-            (sp + cross * (partner - sp), 2 * far_x + c),
-        )
-
-    def down_block(i):
-        j, side = blocks[i]
-        owner, _, half = place(i)
+    def x_copy(i):
+        _, far_x, half, piece = place(i)
+        return remote(
+            comb.at[far_x, half, piece],
+            x_in.at[half, piece],
+            x_send.at[half, piece],
+            x_recv.at[half, piece],
+            (sp, tp_at(2)),
+        )
+
+    def last_copy(i):
+        _, far_x, half, piece = place(i)
+        return remote(
+            last_out.at[half, piece],
+            last_in.at[half, piece],
+            last_send.at[half, piece],
+            last_recv.at[half, piece],
+            (partner, tp),
+        )
+
+    def down_unit(i):
+        owner, _, half, piece = place(i)
         block = 2 * owner + half
         for bit in range(2):
             there = slice(bit * rows, (bit + 1) * rows)
             parts[i, there, :] = jnp.dot(
-                squared[there, :], down_all[block], preferred_element_type=F32
+                squared[there, :], down_all[block, piece], preferred_element_type=F32
             ).astype(BF16)
 
         @pl.when(owner % 2 != c)
@@ -771,47 +873,58 @@
             sib_copy(i).start()
 
     def combine(i):
-        owner, far_x, half = place(i)
+        owner, far_x, half, piece = place(i)
 
         @pl.when(owner % 2 == c)
         def _():
             sib_copy(i).wait_recv()
-            comb[far_x, half] = (
-                parts[i].astype(F32) + sib_in[far_x, half].astype(F32)
+            comb[far_x, half, piece] = (
+                parts[i].astype(F32) + sib_in[far_x, half, piece].astype(F32)
             ).astype(BF16)
-            rs_copy(i, 1)[1].start()
-            turn, copy = rs_copy(i, 0)
-
-            @pl.when(turn == 1)
+
+            @pl.when(far_x != x)
             def _():
-                copy.start()
-
-    for i, (j, side) in enumerate(blocks):
+                x_copy(i).start()
+
+    def settle(i):
+        owner, far_x, half, piece = place(i)
+
+        @pl.when(owner == tp)
+        def _():
+            x_copy(i).wait_recv()
+            last_out[half, piece] = (
+                comb[far_x, half, piece, rows_of(1), :].astype(F32)
+                + x_in[half, piece, rows_of(1), :].astype(F32)
+            ).astype(BF16)
+            last_copy(i).start()
+
+    for i, (j, side, piece) in enumerate(units):
         if side == 0:
-            if j > 0:
-                pump(ups + CHUNKS * j)
+            pump(min(len(events), ups + max(0, i // 2 + 1 - CHUNKS + LEAD)))
         else:
-            for piece in range(CHUNKS):
-                y_arrival(1, j, piece).wait_recv()
-        down_block(i)
+            y_arrival(1, j, piece).wait_recv()
+        down_unit(i)
         if i > 0:
             combine(i - 1)
-    combine(len(blocks) - 1)
+        if i >= SETTLE:
+            settle(i - SETTLE)
+    combine(len(units) - 1)
+    for i in range(len(units) - SETTLE, len(units)):
+        settle(i)
 
     for half in range(2):
-        cols = slice(half * depth, (half + 1) * depth)
-        total = first_ref[:, cols].astype(F32) + comb[x, half, rows_of(0), :].astype(F32)
-        for rel in range(1, 4):
-            there = rs_in.at[rel - 1, half]
+        for piece in range(CHUNKS):
+            start = half * depth + piece * down_piece
+            cols = slice(start, start + down_piece)
+            total = first_ref[:, cols].astype(F32)
+            total = total + comb[x, half, piece, rows_of(0), :].astype(F32)
+            total = total + x_in[half, piece, rows_of(0), :].astype(F32)
+            there = last_in.at[half, piece]
             remote(
-                there,
-                there,
-                rs_send.at[0, 0, 0],
-                rs_recv.at[rel - 1, half],
-                group_at(2 * (rel % 2) + 4 * (rel // 2)),
+                there, there, last_send.at[half, piece], last_recv.at[half, piece], (partner, tp)
             ).wait_recv()
-            total = total + rs_in[rel - 1, half].astype(F32)
-        out_ref[:, cols] = total.astype(BF16)
+            total = total + last_in[half, piece].astype(F32)
+            out_ref[:, cols] = total.astype(BF16)
 
     for k in range(1, m):
         w_copy(k).wait_send()
@@ -824,18 +937,26 @@
         normed_copy(*route).wait_send()
     for stream in range(2):
         for piece in range(CHUNKS):
-            for j in range(1, n // 2):
+            for j in range(1, 3):
                 z_copy(stream, j, piece).wait_send()
+
+            @pl.when(inner)
+            def _():
+                z_copy(stream, 3, piece).wait_send()
+                z_forward(stream, piece).wait_send()
+
             for i in range(n // 2):
                 y_copy(stream, i, piece).wait_send()
+    for copy in near_copies():
+        copy.wait_send()
     for k in range(1, back + 1):
 
-        @pl.when(sp + k < n)
+        @pl.when(z + k < lines)
         def _():
             for copy in state_copies(k):
                 copy.wait_send()
 
-    for i in range(len(blocks)):
+    for i in range(len(units)):
         owner = place(i)[0]
 
         @pl.when(owner % 2 != c)
@@ -844,17 +965,19 @@
 
         @pl.when(owner % 2 == c)
         def _():
-            rs_copy(i, 1)[1].wait_send()
-            turn, copy = rs_copy(i, 0)
-
-            @pl.when(turn == 1)
+
+            @pl.when(place(i)[1] != x)
             def _():
-                copy.wait_send()
-
-
-PUMPS_LOCAL = (0, 1)
-PUMPS_MIX = 2
-PUMPS_NORMED = 5
+                x_copy(i).wait_send()
+
+        @pl.when(owner == tp)
+        def _():
+            last_copy(i).wait_send()
+
+
+PUMPS = (1, 2, 4, 2, 3)
+LEAD = 1
+SETTLE = 8
 
 
 def fused(
@@ -879,9 +1002,9 @@
     depth, hidden_width = up_weight.shape
     width = residual.shape[1]
     own_width = hidden_width // 2
-    back = min(n - 1, (MOST - 2) // rows + 1)
+    lines = n // 2
+    back = min(lines - 1, ((MOST - 2) // rows + 2) // 2)
     dma = pltpu.SemaphoreType.DMA
-    lines = n // 2
     return pl.pallas_call(
         functools.partial(layer_kernel, n, m, back),
         out_shape=jax.ShapeDtypeStruct((rows, width), BF16),
@@ -889,10 +1012,14 @@
         out_specs=pl.BlockSpec(memory_space=pltpu.VMEM),
         scratch_shapes=[
             pltpu.VMEM((n * depth, own_width), BF16),
-            pltpu.VMEM((n, own_width, depth), BF16),
+            pltpu.VMEM((n, CHUNKS, own_width, depth // CHUNKS), BF16),
             pltpu.VMEM((m, heads * DH, width), BF16),
             pltpu.VMEM((heads, DH, DH), BF16),
+            pltpu.VMEM((heads, DH, DH), BF16),
+            pltpu.VMEM((heads, DH, DH), BF16),
             pltpu.VMEM((back, heads, DH, DH), BF16),
+            pltpu.VMEM((heads, 8, DH), F32),
+            pltpu.VMEM((heads, 8, DH), F32),
             pltpu.VMEM((heads, 8, DH), F32),
             pltpu.VMEM((back, heads, 8, DH), F32),
             pltpu.VMEM((heads, rows, DH), F32),
@@ -904,20 +1031,23 @@
             pltpu.VMEM((2, 8, rows), F32),
             pltpu.VMEM((m, 8, rows), F32),
             pltpu.VMEM((2 * rows, own_width), BF16),
-            pltpu.VMEM((n, 2 * rows, depth), BF16),
-            pltpu.VMEM((2, 2, 2 * rows, depth), BF16),
-            pltpu.VMEM((2, 2, 2 * rows, depth), BF16),
-            pltpu.VMEM((3, 2, rows, depth), BF16),
+            pltpu.VMEM((n * CHUNKS, 2 * rows, depth // CHUNKS), BF16),
+            pltpu.VMEM((2, 2, CHUNKS, 2 * rows, depth // CHUNKS), BF16),
+            pltpu.VMEM((2, 2, CHUNKS, 2 * rows, depth // CHUNKS), BF16),
+            pltpu.VMEM((2, CHUNKS, 2 * rows, depth // CHUNKS), BF16),
+            pltpu.VMEM((2, CHUNKS, rows, depth // CHUNKS), BF16),
+            pltpu.VMEM((2, CHUNKS, rows, depth // CHUNKS), BF16),
             dma((m - 1,)),
             dma((m - 1,)),
             dma((2, lines - 1, CHUNKS)),
             dma((2, lines - 1, CHUNKS)),
+            dma((2, CHUNKS)),
             dma((2, lines, CHUNKS)),
             dma((2, lines, CHUNKS)),
-            dma((back,)),
-            dma((back,)),
-            dma((back,)),
-            dma((back,)),
+            dma((2,)),
+            dma((2,)),
+            dma((back, 2)),
+            dma((back, 2)),
             dma((m - 1, heads)),
             dma((m - 1, heads)),
             dma((m - 1,)),
@@ -926,10 +1056,12 @@
             dma((2 * m - 1,)),
             dma((m,)),
             dma((m,)),
-            dma((2, 2)),
-            dma((2, 2)),
-            dma((2, 2, 2)),
-            dma((3, 2)),
+            dma((2, 2, CHUNKS)),
+            dma((2, 2, CHUNKS)),
+            dma((2, CHUNKS)),
+            dma((2, CHUNKS)),
+            dma((2, CHUNKS)),
+            dma((2, CHUNKS)),
         ],
         compiler_params=pltpu.CompilerParams(
             collective_id=0, has_side_effects=True, vmem_limit_bytes=60 * 1024 * 1024

time: 167 us -> 131 us (0.78)
  Pallas kernels: 162 us -> 125 us
    pallas_call x1, Pallas kernels: 162 us -> 125 us  [fused(): pl.pallas_call(functools.partial(layer_kernel, n, m, back), out_shape=jax...]
where the time goes in v2:
time: 131 us; the launch traced here: 129 us
  Pallas kernels  125 us (95%)
  local copies, waits for them, and re-layouts  3.78 us (3%)
    pallas_call x1, Pallas kernels, fused(): pl.pallas_call(functools.partial(layer_kernel, n, m, back), out_shape=jax...  125 us
    unnamed x5, local copies, waits for them, and re-layouts  2.62 us

profile of v2, /device:TPU:24, one launch (start us, length us, event | category | flops | bytes accessed | tf_op | source)
XLA Modules:
  0.0 128.9 jit_solution(5536347105896447686)
XLA Ops:
  0.0 0.0 copy-start.1
  0.0 0.7 copy-done.1
  0.7 0.0 copy-start
  0.7 0.6 broadcast_in_dim.10.cell_gain_ref
  1.2 0.1 copy-done
  1.3 0.6 broadcast_in_dim.11.mixer_gain_ref
  1.9 125.1 %layer.1 = bf16[512,512]{1,0:T(8,128)(2,1)} custom-call(bf16[512,256]{1,0:T(8,128)(2,1)} %q_ref.1, bf16[512,256]{1,0:T(8,128)(2,1)} %k_ref.1, bf16[512,256]{1,0:T(8,128)(2,1)} %v_ref.1, bf16[512,256]{1,0:T(8,128)(2,1)} %og_ref.1, f32[2,512]{1,0:T(2,128)} %bitcast.4, f32[2,512]{1,0:T(2,128)} %bitcast.5, f32[2,512]{1,0:T(2,128)} %bitcast.6, s32[1,512]{1,0:T(1,128)} %bitcast.7, ...), custom_call_target="tpu_custom_call" | custom-call | tf_op jit(solution)/shard_map/layer/pallas_call | solution.py:1008
  127.0 1.9 %copy.16 = bf16[512,512]{1,0:T(8,128)(2,1)} copy(bf16[512,512]{1,0:T(8,128)(2,1)} %layer.1) | data formatting | bytes 1048576
Async XLA Ops:
  0.0 0.7 copy-start.1
  0.7 0.7 copy-start

commit v3 on v2

--- a/solution.py
+++ b/solution.py
@@ -215,6 +215,7 @@
 F32 = jnp.float32
 BF16 = jnp.bfloat16
 CHUNKS = 2
+SUBS = 2
 
 
 def to_columns(rows):
@@ -283,6 +284,7 @@
     x_in,
     last_out,
     last_in,
+    diag_in,
     w_send,
     w_recv,
     z_send,
@@ -306,6 +308,7 @@
     sib_recv,
     x_send,
     x_recv,
+    diag_recv,
     last_send,
     last_recv,
 ):
@@ -314,7 +317,8 @@
     depth, hidden_width = up_ref.shape
     own_width = hidden_width // 2
     width = resid_ref.shape[1]
-    up_piece, down_piece = depth // CHUNKS, depth // CHUNKS
+    up_piece, down_piece = depth // (CHUNKS * SUBS), depth // CHUNKS
+    deep_piece = own_width // SUBS
     z, y, lines = sp // 2, sp % 2, n // 2
     p, x, c = z % 2, tp // 2, tp % 2
 
@@ -334,7 +338,8 @@
         pl.semaphore_signal(barrier, device_id=((sp + k) % n, tp), device_id_type=MESH)
     for k in range(1, m):
         pl.semaphore_signal(barrier, device_id=(sp, (tp + k) % m), device_id_type=MESH)
-    pl.semaphore_wait(barrier, n + m - 2)
+    pl.semaphore_signal(barrier, device_id=(partner, tp_at(2)), device_id_type=MESH)
+    pl.semaphore_wait(barrier, n + m - 1)
 
     def remote(src, dst, send_sem, recv_sem, device):
         return pltpu.make_async_remote_copy(
@@ -366,14 +371,16 @@
         if stream == 0:
             start = pl.multiple_of(block * depth + piece * up_piece, up_piece)
             return up_all.at[pl.ds(start, up_piece), :]
-        return down_all.at[block, piece]
+        deep = pl.ds(piece % SUBS * deep_piece, deep_piece)
+        return down_all.at[block, piece // SUBS, deep]
 
     def own_piece(stream, half, piece):
         if stream == 0:
             lanes = pl.ds(pl.multiple_of(half * own_width, own_width), own_width)
             return up_ref.at[pl.ds(piece * up_piece, up_piece), lanes]
-        deep = pl.ds(pl.multiple_of(half * own_width, own_width), own_width)
-        return down_ref.at[deep, pl.ds(piece * down_piece, down_piece)]
+        start = pl.multiple_of(half * own_width + piece % SUBS * deep_piece, deep_piece)
+        cols = pl.ds(piece // SUBS * down_piece, down_piece)
+        return down_ref.at[pl.ds(start, deep_piece), cols]
 
     def z_copy(stream, j, piece):
         return remote(
@@ -427,11 +434,26 @@
         )
 
     order = ((1, 0), (1, 1), (2, 0), (3, 0), (2, 1), (3, 1))
-    events = [(stream, j, piece) for stream in range(2) for j, piece in order]
+    down_order = ((1, 0), (2, 0), (3, 0), (1, 1), (2, 1), (3, 1))
+    events = [
+        (stream, j, SUBS * piece + i)
+        for stream in range(2)
+        for j, piece in (order, down_order)[stream]
+        for i in range(SUBS)
+    ]
+
+    def z_start(stream, j, piece):
+        for i in range(SUBS):
+            z_copy(stream, j, SUBS * piece + i).start()
+
+    def y_start(stream, piece):
+        for i in range(SUBS):
+            y_copy(stream, 0, SUBS * piece + i).start()
+
     done = [0]
 
     def pump(until):
-        while done[0] < until:
+        while done[0] < min(SUBS * until, len(events)):
             event = done[0]
             stream, j, piece = events[event]
             done[0] += 1
@@ -516,14 +538,14 @@
 
     for copy in near_copies():
         copy.start()
-    z_copy(0, 1, 0).start()
+    z_start(0, 1, 0)
 
     @pl.when(inner)
     def _():
-        z_copy(0, 3, 0).start()
+        z_start(0, 3, 0)
 
     for piece in range(CHUNKS):
-        y_copy(0, 0, piece).start()
+        y_start(0, piece)
 
     for k in range(1, back + 1):
 
@@ -537,6 +559,10 @@
     for piece in range(CHUNKS):
         cols = slice(piece * down_piece, (piece + 1) * down_piece)
         down_all[sp, piece] = down_ref[half_lanes, cols]
+
+    @pl.when(x == z // 2)
+    def _():
+        diag_in[...] = jnp.zeros(diag_in.shape, BF16)
 
     step = min(rows, 256)
     locals_of = []
@@ -593,8 +619,8 @@
             for copy in state_copies(k):
                 copy.start()
 
-    z_copy(0, 1, 1).start()
-    z_copy(0, 2, 0).start()
+    z_start(0, 1, 1)
+    z_start(0, 2, 0)
     for k in range(1, back + 1):
 
         @pl.when(z >= k)
@@ -658,7 +684,7 @@
         cell = numer / jnp.maximum(jnp.abs(denom), 1.0)
         square_sum = square_sum + cell * cell
         gated = jax.nn.sigmoid(og_ref[:, mine].astype(F32))
-        y_all[tp, :, mine] = (gated * cell * cell_gain_ref[:, mine].astype(F32)).astype(BF16)
+        y_all[tp, :, mine] = (gated * cell * cell_gain_ref[mine].astype(F32)[None, :]).astype(BF16)
         for k in range(1, 3):
             mix_copy(k, h).start()
     squares_out[...] = to_rows(jnp.sum(square_sum, axis=1, keepdims=True))
@@ -681,7 +707,7 @@
     @pl.when(inner)
     def _():
         for j in (2, 3):
-            z_copy(0, j, 1).start()
+            z_start(0, j, 1)
 
     for h in range(heads):
         mix_arrival(2, h).wait_recv()
@@ -710,7 +736,7 @@
     def rows_of(bit):
         return pl.ds(pl.multiple_of(plane(bit) * rows, rows), rows)
 
-    normed[rows_of(0), here] = (first * mixer_gain_ref[...].astype(F32)).astype(BF16)
+    normed[rows_of(0), here] = (first * mixer_gain_ref[...].astype(F32)[None, :]).astype(BF16)
 
     def group_at(bits):
         return (sp + (bits // 4) * (partner - sp), tp_at(bits % 4))
@@ -754,11 +780,10 @@
 
     @pl.when(jnp.logical_not(inner))
     def _():
-        z_copy(0, 2, 1).start()
-
-    y_copy(1, 0, 0).start()
+        z_start(0, 2, 1)
+
+    y_start(1, 0)
     pump(PUMPS[2])
-    y_copy(1, 0, 1).start()
     normed_arrival(2).wait_recv()
     normed_copy(2, 1).start()
     normed_arrival(4).wait_recv()
@@ -771,24 +796,19 @@
     @pl.when(inner)
     def _():
         for j in (2, 3):
-            z_copy(1, j, 0).start()
+            z_start(1, j, 0)
 
     pump(ups)
 
-    z_copy(1, 1, 0).start()
+    z_start(1, 1, 0)
 
     @pl.when(jnp.logical_not(inner))
     def _():
-        z_copy(1, 2, 0).start()
-
-    z_copy(1, 1, 1).start()
-
-    @pl.when(jnp.logical_not(inner))
-    def _():
-        z_copy(1, 2, 1).start()
-
+        z_start(1, 2, 0)
+
+    y_start(1, 1)
     for i in range(n // 2):
-        for piece in range(CHUNKS):
+        for piece in range(CHUNKS * SUBS):
             y_arrival(0, i, piece).wait_recv()
 
     tile = min(own_width, 256)
@@ -808,10 +828,6 @@
     up_half(0, total)
     pump(ups + 1)
 
-    @pl.when(inner)
-    def _():
-        for j in (2, 3):
-            z_copy(1, j, 1).start()
 
     normed_arrival(6).wait_recv()
     normed_copy(6, 1).start()
@@ -819,9 +835,15 @@
     normed_arrival(7).wait_recv()
     sums_copy(4).wait_recv()
     up_half(1, sums_in[3])
-    pump(ups + PUMPS[3])
-
-    pairs = [(0, piece) for piece in range(CHUNKS)] + list(order)
+    for j in (1, 2):
+        z_start(1, j, 1)
+
+    @pl.when(inner)
+    def _():
+        z_start(1, 3, 1)
+
+
+    pairs = [(0, piece) for piece in range(CHUNKS)] + list(down_order)
     units = [(j, side, piece) for j, piece in pairs for side in range(2)]
 
     def place(i):
@@ -829,88 +851,111 @@
         owner = z_at(j)
         return owner, owner // 2, y + side * (1 - 2 * y), piece
 
-    def sib_copy(i):
+    def sib_copy(i, bit):
         _, far_x, half, piece = place(i)
-        return remote(
-            parts.at[i],
-            sib_in.at[far_x, half, piece],
-            sib_send.at[far_x, half, piece],
-            sib_recv.at[far_x, half, piece],
+        here = pl.ds(bit * rows if isinstance(bit, int) else pl.multiple_of(bit * rows, rows), rows)
+        return remote(
+            parts.at[i, here],
+            sib_in.at[far_x, half, piece, here],
+            sib_send.at[far_x, half, piece, bit],
+            sib_recv.at[far_x, half, piece, bit],
             (sp, tp_at(1)),
         )
 
-    def x_copy(i):
+    def x_copy(i, cross):
         _, far_x, half, piece = place(i)
-        return remote(
-            comb.at[far_x, half, piece],
-            x_in.at[half, piece],
-            x_send.at[half, piece],
-            x_recv.at[half, piece],
-            (sp, tp_at(2)),
+        late = cross == 1 and units[i][0] > 1
+        return remote(
+            comb.at[far_x, half, piece, rows_of(cross)],
+            diag_in.at[half, piece] if late else x_in.at[half, piece, rows_of(cross)],
+            x_send.at[half, piece, cross],
+            diag_recv.at[half, piece] if late else x_recv.at[half, piece, cross],
+            (partner if late else sp, tp_at(2)),
         )
 
     def last_copy(i):
         _, far_x, half, piece = place(i)
-        return remote(
-            last_out.at[half, piece],
+        late = units[i][0] > 1
+        return remote(
+            comb.at[far_x, half, piece, rows_of(1)] if late else last_out.at[half, piece],
             last_in.at[half, piece],
             last_send.at[half, piece],
             last_recv.at[half, piece],
             (partner, tp),
         )
 
-    def down_unit(i):
-        owner, _, half, piece = place(i)
-        block = 2 * owner + half
+    def down_units(*which):
+        deep = [down_all[2 * place(i)[0] + place(i)[2], place(i)[3]] for i in which]
+        deep = jnp.concatenate(deep, axis=1)
         for bit in range(2):
-            there = slice(bit * rows, (bit + 1) * rows)
-            parts[i, there, :] = jnp.dot(
-                squared[there, :], down_all[block, piece], preferred_element_type=F32
-            ).astype(BF16)
-
-        @pl.when(owner % 2 != c)
-        def _():
-            sib_copy(i).start()
+            here = slice(bit * rows, (bit + 1) * rows)
+            wide = jnp.dot(squared[here, :], deep, preferred_element_type=F32).astype(BF16)
+            for k, i in enumerate(which):
+                parts[i, here, :] = wide[:, k * down_piece : (k + 1) * down_piece]
+        for i in which:
+
+            @pl.when(place(i)[0] % 2 != c)
+            def _():
+                for bit in range(2):
+                    sib_copy(i, bit).start()
 
     def combine(i):
         owner, far_x, half, piece = place(i)
 
         @pl.when(owner % 2 == c)
         def _():
-            sib_copy(i).wait_recv()
-            comb[far_x, half, piece] = (
-                parts[i].astype(F32) + sib_in[far_x, half, piece].astype(F32)
-            ).astype(BF16)
-
-            @pl.when(far_x != x)
-            def _():
-                x_copy(i).start()
+            for cross in (1, 0):
+                here = rows_of(cross)
+                sib_copy(i, plane(cross)).wait_recv()
+                comb[far_x, half, piece, here, :] = (
+                    parts[i, here, :].astype(F32)
+                    + sib_in[far_x, half, piece, here, :].astype(F32)
+                ).astype(BF16)
+
+                @pl.when(far_x != x)
+                def _():
+                    x_copy(i, cross).start()
+
+                if cross == 1 and units[i][0] > 1:
+
+                    @pl.when(far_x == x)
+                    def _():
+                        last_copy(i).start()
 
     def settle(i):
         owner, far_x, half, piece = place(i)
 
         @pl.when(owner == tp)
         def _():
-            x_copy(i).wait_recv()
+            x_copy(i, 1).wait_recv()
             last_out[half, piece] = (
                 comb[far_x, half, piece, rows_of(1), :].astype(F32)
                 + x_in[half, piece, rows_of(1), :].astype(F32)
             ).astype(BF16)
             last_copy(i).start()
 
-    for i, (j, side, piece) in enumerate(units):
-        if side == 0:
-            pump(min(len(events), ups + max(0, i // 2 + 1 - CHUNKS + LEAD)))
-        else:
-            y_arrival(1, j, piece).wait_recv()
-        down_unit(i)
-        if i > 0:
-            combine(i - 1)
-        if i >= SETTLE:
-            settle(i - SETTLE)
-    combine(len(units) - 1)
-    for i in range(len(units) - SETTLE, len(units)):
-        settle(i)
+    early = [i for i, unit in enumerate(units) if unit[0] < 2]
+    settling = {len(pairs) - 4 + i // 2: early[i : i + 2] for i in range(0, len(early), 2)}
+    waiting = []
+    for k, (j, piece) in enumerate(pairs):
+        pump(ups + max(0, k + 1 - CHUNKS + LEAD))
+        ready = (2 * k, 2 * k + 1)
+        if k >= SINGLES:
+            down_units(ready[0])
+            combine(ready[0])
+        for i in range(SUBS):
+            y_arrival(1, j, SUBS * piece + i).wait_recv()
+        down_units(*ready[1 if k >= SINGLES else 0 :])
+        for i in waiting:
+            combine(i)
+        waiting = list(ready) if k < 2 else []
+        if k >= 2:
+            for i in ready[1 if k >= SINGLES else 0 :]:
+                combine(i)
+        for i in settling.get(k, ()):
+            settle(i)
+    for i in waiting:
+        combine(i)
 
     for half in range(2):
         for piece in range(CHUNKS):
@@ -918,12 +963,27 @@
             cols = slice(start, start + down_piece)
             total = first_ref[:, cols].astype(F32)
             total = total + comb[x, half, piece, rows_of(0), :].astype(F32)
-            total = total + x_in[half, piece, rows_of(0), :].astype(F32)
-            there = last_in.at[half, piece]
-            remote(
-                there, there, last_send.at[half, piece], last_recv.at[half, piece], (partner, tp)
-            ).wait_recv()
-            total = total + last_in[half, piece].astype(F32)
+
+            def landed(ref, send_sem, recv_sem):
+                remote(ref, ref, send_sem, recv_sem, (partner, tp)).wait_recv()
+                return ref[...].astype(F32)
+
+            total = total + landed(
+                x_in.at[half, piece, rows_of(0)],
+                x_send.at[half, piece, 0],
+                x_recv.at[half, piece, 0],
+            )
+            total = total + landed(
+                last_in.at[half, piece], last_send.at[half, piece], last_recv.at[half, piece]
+            )
+
+            @pl.when(x != z // 2)
+            def _():
+                landed(
+                    diag_in.at[half, piece], x_send.at[half, piece, 0], diag_recv.at[half, piece]
+                )
+
+            total = total + diag_in[half, piece].astype(F32)
             out_ref[:, cols] = total.astype(BF16)
 
     for k in range(1, m):
@@ -936,7 +996,7 @@
     for route in routes:
         normed_copy(*route).wait_send()
     for stream in range(2):
-        for piece in range(CHUNKS):
+        for piece in range(CHUNKS * SUBS):
             for j in range(1, 3):
                 z_copy(stream, j, piece).wait_send()
 
@@ -961,14 +1021,13 @@
 
         @pl.when(owner % 2 != c)
         def _():
-            sib_copy(i).wait_send()
-
-        @pl.when(owner % 2 == c)
+            for bit in range(2):
+                sib_copy(i, bit).wait_send()
+
+        @pl.when((owner % 2 == c) & (place(i)[1] != x))
         def _():
-
-            @pl.when(place(i)[1] != x)
-            def _():
-                x_copy(i).wait_send()
+            for cross in range(2):
+                x_copy(i, cross).wait_send()
 
         @pl.when(owner == tp)
         def _():
@@ -977,7 +1036,7 @@
 
 PUMPS = (1, 2, 4, 2, 3)
 LEAD = 1
-SETTLE = 8
+SINGLES = 3
 
 
 def fused(
@@ -1037,13 +1096,14 @@
             pltpu.VMEM((2, CHUNKS, 2 * rows, depth // CHUNKS), BF16),
             pltpu.VMEM((2, CHUNKS, rows, depth // CHUNKS), BF16),
             pltpu.VMEM((2, CHUNKS, rows, depth // CHUNKS), BF16),
+            pltpu.VMEM((2, CHUNKS, rows, depth // CHUNKS), BF16),
             dma((m - 1,)),
             dma((m - 1,)),
-            dma((2, lines - 1, CHUNKS)),
-            dma((2, lines - 1, CHUNKS)),
-            dma((2, CHUNKS)),
-            dma((2, lines, CHUNKS)),
-            dma((2, lines, CHUNKS)),
+            dma((2, lines - 1, CHUNKS * SUBS)),
+            dma((2, lines - 1, CHUNKS * SUBS)),
+            dma((2, CHUNKS * SUBS)),
+            dma((2, lines, CHUNKS * SUBS)),
+            dma((2, lines, CHUNKS * SUBS)),
             dma((2,)),
             dma((2,)),
             dma((back, 2)),
@@ -1056,9 +1116,10 @@
             dma((2 * m - 1,)),
             dma((m,)),
             dma((m,)),
-            dma((2, 2, CHUNKS)),
-            dma((2, 2, CHUNKS)),
-            dma((2, CHUNKS)),
+            dma((2, 2, CHUNKS, 2)),
+            dma((2, 2, CHUNKS, 2)),
+            dma((2, CHUNKS, 2)),
+            dma((2, CHUNKS, 2)),
             dma((2, CHUNKS)),
             dma((2, CHUNKS)),
             dma((2, CHUNKS)),
@@ -1077,8 +1138,8 @@
         input_gate_log.T,
         document[None, :],
         residual,
-        cell_norm_gain[None, :],
-        mixer_norm_gain[None, :],
+        cell_norm_gain,
+        mixer_norm_gain,
         output_weight,
         up_weight,
         down_weight,

time: 131 us -> 124 us (0.947); the launches traced: 129 us -> 124 us
  Pallas kernels: 125 us -> 122 us
  local copies, waits for them, and re-layouts: 3.78 us -> 1.87 us
    pallas_call x1, Pallas kernels: 125 us -> 122 us  [fused(): pl.pallas_call(functools.partial(layer_kernel, n, m, back), out_shape=jax...]
    unnamed x5 -> x1, local copies, waits for them, and re-layouts: 2.62 us -> 1.87 us
where the time goes in v3:
time: 124 us
  Pallas kernels  122 us (98%)
  local copies, waits for them, and re-layouts  1.87 us (2%)
    pallas_call x1, Pallas kernels, fused(): pl.pallas_call(functools.partial(layer_kernel, n, m, back), out_shape=jax...  122 us

profile of v3, /device:TPU:24, one launch (start us, length us, event | category | flops | bytes accessed | tf_op | source)
XLA Modules:
  0.0 123.6 jit_solution(16709198438444996908)
XLA Ops:
  0.0 121.7 %layer.1 = bf16[512,512]{1,0:T(8,128)(2,1)} custom-call(bf16[512,256]{1,0:T(8,128)(2,1)} %q_ref.1, bf16[512,256]{1,0:T(8,128)(2,1)} %k_ref.1, bf16[512,256]{1,0:T(8,128)(2,1)} %v_ref.1, bf16[512,256]{1,0:T(8,128)(2,1)} %og_ref.1, f32[2,512]{1,0:T(2,128)} %bitcast.4, f32[2,512]{1,0:T(2,128)} %bitcast.5, f32[2,512]{1,0:T(2,128)} %bitcast.6, s32[1,512]{1,0:T(1,128)} %bitcast.7, ...), custom_call_target="tpu_custom_call" | custom-call | tf_op jit(solution)/shard_map/layer/pallas_call | solution.py:1067
  121.7 1.9 %copy.16 = bf16[512,512]{1,0:T(8,128)(2,1)} copy(bf16[512,512]{1,0:T(8,128)(2,1)} %layer.1) | data formatting | bytes 1048576

commit v4 on v3

--- a/solution.py
+++ b/solution.py
@@ -243,20 +243,29 @@
     n,
     m,
     back,
-    q_ref,
-    k_ref,
-    v_ref,
-    og_ref,
+    q_hbm,
+    k_hbm,
+    v_hbm,
+    og_hbm,
     forget_ref,
     extra_ref,
     input_ref,
     doc_ref,
-    resid_ref,
+    resid_hbm,
     cell_gain_ref,
     mixer_gain_ref,
+    wout_hbm,
+    up_hbm,
+    down_hbm,
+    out_hbm,
+    k_ref,
+    v_ref,
+    up_ref,
+    q_ref,
     wout_ref,
-    up_ref,
     down_ref,
+    og_ref,
+    resid_ref,
     out_ref,
     up_all,
     down_all,
@@ -311,7 +320,26 @@
     diag_recv,
     last_send,
     last_recv,
+    load_sem,
+    store_sem,
 ):
+    loads = (
+        (up_hbm, up_ref),
+        (k_hbm, k_ref),
+        (v_hbm, v_ref),
+        (wout_hbm, wout_ref),
+        (q_hbm, q_ref),
+        (down_hbm, down_ref),
+        (og_hbm, og_ref),
+        (resid_hbm, resid_ref),
+    )
+
+    def fetch(ref):
+        at = [dst is ref for _, dst in loads].index(True)
+        return pltpu.make_async_copy(*loads[at], load_sem.at[at])
+
+    for _, ref in loads:
+        fetch(ref).start()
     sp, tp = lax.axis_index("sp"), lax.axis_index("tp")
     rows, heads = q_ref.shape[0], q_ref.shape[1] // DH
     depth, hidden_width = up_ref.shape
@@ -452,21 +480,40 @@
 
     done = [0]
 
+    def relay(event):
+        stream, j, piece = events[event]
+        z_arrival(stream, j, piece).wait_recv()
+        y_copy(stream, j, piece).start()
+        if j == 1:
+
+            @pl.when(inner)
+            def _():
+                z_forward(stream, piece).start()
+
     def pump(until):
         while done[0] < min(SUBS * until, len(events)):
             event = done[0]
-            stream, j, piece = events[event]
+            relay(event)
             done[0] += 1
-            z_arrival(stream, j, piece).wait_recv()
-            y_copy(stream, j, piece).start()
-            if j == 1:
-
-                @pl.when(inner)
-                def _():
-                    z_forward(stream, piece).start()
+
+    def relay_when(condition, down_events):
+        if down_events:
+
+            @pl.when(condition)
+            def _():
+                for event in down_events:
+                    relay(SUBS * ups + event)
 
     ups = len(order)
 
+    fetch(up_ref).wait()
+    z_start(0, 1, 0)
+
+    @pl.when(inner)
+    def _():
+        z_start(0, 3, 0)
+
+    fetch(wout_ref).wait()
     for k in range(1, m):
         w_copy(k).start()
 
@@ -505,6 +552,8 @@
     columns = to_columns(packed)
     doc_col = columns[:, 2 * heads : 2 * heads + 1]
     line = lax.broadcasted_iota(jnp.int32, (8, DH), 0)
+    fetch(k_ref).wait()
+    fetch(v_ref).wait()
     for h in range(heads):
         mine = slice(h * DH, (h + 1) * DH)
         weighted = k_ref[:, mine].astype(F32) * columns[:, heads + h : heads + h + 1]
@@ -538,12 +587,6 @@
 
     for copy in near_copies():
         copy.start()
-    z_start(0, 1, 0)
-
-    @pl.when(inner)
-    def _():
-        z_start(0, 3, 0)
-
     for piece in range(CHUNKS):
         y_start(0, piece)
 
@@ -554,6 +597,7 @@
             tail_in[k - 1] = jnp.zeros((heads, 8, DH), F32)
             state_in[k - 1] = jnp.zeros((heads, DH, DH), BF16)
 
+    fetch(down_ref).wait()
     half_lanes = pl.ds(pl.multiple_of(p * own_width, own_width), own_width)
     up_all[pl.ds(pl.multiple_of(sp * depth, depth), depth), :] = up_ref[:, half_lanes]
     for piece in range(CHUNKS):
@@ -564,6 +608,7 @@
     def _():
         diag_in[...] = jnp.zeros(diag_in.shape, BF16)
 
+    fetch(q_ref).wait()
     step = min(rows, 256)
     locals_of = []
     for h in range(heads):
@@ -644,6 +689,7 @@
             there, there, mix_send.at[k - 1, h], mix_recv.at[k - 1, h], (sp, tp_at(k))
         )
 
+    fetch(og_ref).wait()
     first_doc = document[:, 0:1]
     square_sum = jnp.zeros((rows, DH), F32)
     for h in range(heads):
@@ -725,6 +771,7 @@
     for k in range(1, m):
         square_copy(k).wait_recv()
         squares = squares + squares_in[k - 1]
+    fetch(resid_ref).wait()
     inverse = lax.rsqrt(to_columns(squares)[:, 0:1] / (heads * DH * m) + EPS)
     first = (resid_ref[...].astype(F32) + attn * inverse).astype(BF16)
     first_ref[...] = first
@@ -934,15 +981,18 @@
             ).astype(BF16)
             last_copy(i).start()
 
-    early = [i for i, unit in enumerate(units) if unit[0] < 2]
-    settling = {len(pairs) - 4 + i // 2: early[i : i + 2] for i in range(0, len(early), 2)}
     waiting = []
     for k, (j, piece) in enumerate(pairs):
-        pump(ups + max(0, k + 1 - CHUNKS + LEAD))
+        relay_when(z + 1 < lines, LEADS.get(k))
+        relay_when(z + 1 == lines, FAR_LEADS.get(k))
         ready = (2 * k, 2 * k + 1)
         if k >= SINGLES:
             down_units(ready[0])
             combine(ready[0])
+        relay_when(z + 1 == lines, FAR_MIDS.get(k))
+        if k in SETTLES:
+            settle(2 * SETTLES[k])
+            settle(2 * SETTLES[k] + 1)
         for i in range(SUBS):
             y_arrival(1, j, SUBS * piece + i).wait_recv()
         down_units(*ready[1 if k >= SINGLES else 0 :])
@@ -952,10 +1002,16 @@
         if k >= 2:
             for i in ready[1 if k >= SINGLES else 0 :]:
                 combine(i)
-        for i in settling.get(k, ()):
-            settle(i)
+        relay_when(z + 1 == lines, FAR_TRAILS.get(k))
     for i in waiting:
         combine(i)
+
+    def store(half, piece):
+        start = half * depth + piece * down_piece
+        cols = pl.ds(start, down_piece)
+        return pltpu.make_async_copy(
+            out_ref.at[:, cols], out_hbm.at[:, cols], store_sem.at[half, piece]
+        )
 
     for half in range(2):
         for piece in range(CHUNKS):
@@ -985,6 +1041,7 @@
 
             total = total + diag_in[half, piece].astype(F32)
             out_ref[:, cols] = total.astype(BF16)
+            store(half, piece).start()
 
     for k in range(1, m):
         w_copy(k).wait_send()
@@ -1033,9 +1090,17 @@
         def _():
             last_copy(i).wait_send()
 
+    for half in range(2):
+        for piece in range(CHUNKS):
+            store(half, piece).wait()
+
 
 PUMPS = (1, 2, 4, 2, 3)
-LEAD = 1
+LEADS = {2: (2, 3), 3: (4, 5), 4: (6, 7), 5: (8, 9), 6: (10, 11)}
+FAR_LEADS = {2: (2, 3)}
+SETTLES = {3: 0, 4: 1, 5: 2, 7: 5}
+FAR_MIDS = {3: (6, 7), 4: (8, 9), 6: (10,)}
+FAR_TRAILS = {3: (4, 5), 6: (11,)}
 SINGLES = 3
 
 
@@ -1064,12 +1129,23 @@
     lines = n // 2
     back = min(lines - 1, ((MOST - 2) // rows + 2) // 2)
     dma = pltpu.SemaphoreType.DMA
+    near, far = pltpu.VMEM, pl.ANY
+    spaces = [far] * 4 + [near] * 4 + [far, near, near, far, far, far]
     return pl.pallas_call(
         functools.partial(layer_kernel, n, m, back),
         out_shape=jax.ShapeDtypeStruct((rows, width), BF16),
-        in_specs=[pl.BlockSpec(memory_space=pltpu.VMEM)] * 14,
-        out_specs=pl.BlockSpec(memory_space=pltpu.VMEM),
+        in_specs=[pl.BlockSpec(memory_space=space) for space in spaces],
+        out_specs=pl.BlockSpec(memory_space=pl.ANY),
         scratch_shapes=[
+            pltpu.VMEM(keys.shape, BF16),
+            pltpu.VMEM(values.shape, BF16),
+            pltpu.VMEM(up_weight.shape, BF16),
+            pltpu.VMEM(queries.shape, BF16),
+            pltpu.VMEM(output_weight.shape, BF16),
+            pltpu.VMEM(down_weight.shape, BF16),
+            pltpu.VMEM(output_gate_logits.shape, BF16),
+            pltpu.VMEM(residual.shape, BF16),
+            pltpu.VMEM((rows, width), BF16),
             pltpu.VMEM((n * depth, own_width), BF16),
             pltpu.VMEM((n, CHUNKS, own_width, depth // CHUNKS), BF16),
             pltpu.VMEM((m, heads * DH, width), BF16),
@@ -1123,6 +1199,8 @@
             dma((2, CHUNKS)),
             dma((2, CHUNKS)),
             dma((2, CHUNKS)),
+            dma((8,)),
+            dma((2, CHUNKS)),
         ],
         compiler_params=pltpu.CompilerParams(
             collective_id=0, has_side_effects=True, vmem_limit_bytes=60 * 1024 * 1024

time: 124 us -> 121 us (0.976)
  the two profiles are of different devices: /device:TPU:24 before, /device:TPU:25 now
where the time goes in v4:
time: 121 us; the launch traced here: 120 us
  Pallas kernels  119 us (98%)
  local copies, waits for them, and re-layouts  1.87 us (2%)
    pallas_call x1, Pallas kernels, fused(): pl.pallas_call(functools.partial(layer_kernel, n, m, back), out_shape=jax...  119 us

profile of v4, /device:TPU:25, one launch (start us, length us, event | category | flops | bytes accessed | tf_op | source)
XLA Modules:
  0.0 120.4 jit_solution(13359918939031026360)
XLA Ops:
  0.0 118.5 %layer.1 = bf16[512,512]{1,0:T(8,128)(2,1)} custom-call(bf16[512,256]{1,0:T(8,128)(2,1)} %q_hbm.1, bf16[512,256]{1,0:T(8,128)(2,1)} %k_hbm.1, bf16[512,256]{1,0:T(8,128)(2,1)} %v_hbm.1, bf16[512,256]{1,0:T(8,128)(2,1)} %og_hbm.1, f32[2,512]{1,0:T(2,128)} %bitcast.4, f32[2,512]{1,0:T(2,128)} %bitcast.5, f32[2,512]{1,0:T(2,128)} %bitcast.6, s32[1,512]{1,0:T(1,128)} %bitcast.7, ...), custom_call_target="tpu_custom_call" | custom-call | tf_op jit(solution)/shard_map/layer/pallas_call | solution.py:1134
  118.5 1.9 %copy.16 = bf16[512,512]{1,0:T(8,128)(2,1)} copy(bf16[512,512]{1,0:T(8,128)(2,1)} %layer.1) | data formatting | bytes 1048576

commit v5 on v4

--- a/solution.py
+++ b/solution.py
@@ -659,9 +659,9 @@
 
     for k in range(1, back + 1):
 
-        @pl.when(z + k < lines)
+        @pl.when(z + back + 1 - k < lines)
         def _():
-            for copy in state_copies(k):
+            for copy in state_copies(back + 1 - k):
                 copy.start()
 
     z_start(0, 1, 1)
@@ -1006,43 +1006,6 @@
     for i in waiting:
         combine(i)
 
-    def store(half, piece):
-        start = half * depth + piece * down_piece
-        cols = pl.ds(start, down_piece)
-        return pltpu.make_async_copy(
-            out_ref.at[:, cols], out_hbm.at[:, cols], store_sem.at[half, piece]
-        )
-
-    for half in range(2):
-        for piece in range(CHUNKS):
-            start = half * depth + piece * down_piece
-            cols = slice(start, start + down_piece)
-            total = first_ref[:, cols].astype(F32)
-            total = total + comb[x, half, piece, rows_of(0), :].astype(F32)
-
-            def landed(ref, send_sem, recv_sem):
-                remote(ref, ref, send_sem, recv_sem, (partner, tp)).wait_recv()
-                return ref[...].astype(F32)
-
-            total = total + landed(
-                x_in.at[half, piece, rows_of(0)],
-                x_send.at[half, piece, 0],
-                x_recv.at[half, piece, 0],
-            )
-            total = total + landed(
-                last_in.at[half, piece], last_send.at[half, piece], last_recv.at[half, piece]
-            )
-
-            @pl.when(x != z // 2)
-            def _():
-                landed(
-                    diag_in.at[half, piece], x_send.at[half, piece, 0], diag_recv.at[half, piece]
-                )
-
-            total = total + diag_in[half, piece].astype(F32)
-            out_ref[:, cols] = total.astype(BF16)
-            store(half, piece).start()
-
     for k in range(1, m):
         w_copy(k).wait_send()
         square_copy(k).wait_send()
@@ -1072,6 +1035,43 @@
         def _():
             for copy in state_copies(k):
                 copy.wait_send()
+
+    def store(half, piece):
+        start = half * depth + piece * down_piece
+        cols = pl.ds(start, down_piece)
+        return pltpu.make_async_copy(
+            out_ref.at[:, cols], out_hbm.at[:, cols], store_sem.at[half, piece]
+        )
+
+    for half in range(2):
+        for piece in range(CHUNKS):
+            start = half * depth + piece * down_piece
+            cols = slice(start, start + down_piece)
+            total = first_ref[:, cols].astype(F32)
+            total = total + comb[x, half, piece, rows_of(0), :].astype(F32)
+
+            def landed(ref, send_sem, recv_sem):
+                remote(ref, ref, send_sem, recv_sem, (partner, tp)).wait_recv()
+                return ref[...].astype(F32)
+
+            total = total + landed(
+                x_in.at[half, piece, rows_of(0)],
+                x_send.at[half, piece, 0],
+                x_recv.at[half, piece, 0],
+            )
+            total = total + landed(
+                last_in.at[half, piece], last_send.at[half, piece], last_recv.at[half, piece]
+            )
+
+            @pl.when(x != z // 2)
+            def _():
+                landed(
+                    diag_in.at[half, piece], x_send.at[half, piece, 0], diag_recv.at[half, piece]
+                )
+
+            total = total + diag_in[half, piece].astype(F32)
+            out_ref[:, cols] = total.astype(BF16)
+            store(half, piece).start()
 
     for i in range(len(units)):
         owner = place(i)[0]

time: 121 us -> 121 us (level)
  no operation moved by 1% of the time
where the time goes in v5:
time: 121 us; the launch traced here: 120 us
  Pallas kernels  119 us (98%)
  local copies, waits for them, and re-layouts  1.87 us (2%)
    pallas_call x1, Pallas kernels, fused(): pl.pallas_call(functools.partial(layer_kernel, n, m, back), out_shape=jax...  119 us

profile of v5, /device:TPU:25, one launch (start us, length us, event | category | flops | bytes accessed | tf_op | source)
XLA Modules:
  0.0 120.4 jit_solution(3764949055860798420)
XLA Ops:
  0.0 118.5 %layer.1 = bf16[512,512]{1,0:T(8,128)(2,1)} custom-call(bf16[512,256]{1,0:T(8,128)(2,1)} %q_hbm.1, bf16[512,256]{1,0:T(8,128)(2,1)} %k_hbm.1, bf16[512,256]{1,0:T(8,128)(2,1)} %v_hbm.1, bf16[512,256]{1,0:T(8,128)(2,1)} %og_hbm.1, f32[2,512]{1,0:T(2,128)} %bitcast.4, f32[2,512]{1,0:T(2,128)} %bitcast.5, f32[2,512]{1,0:T(2,128)} %bitcast.6, s32[1,512]{1,0:T(1,128)} %bitcast.7, ...), custom_call_target="tpu_custom_call" | custom-call | tf_op jit(solution)/shard_map/layer/pallas_call | solution.py:1134
  118.5 1.9 %copy.16 = bf16[512,512]{1,0:T(8,128)(2,1)} copy(bf16[512,512]{1,0:T(8,128)(2,1)} %layer.1) | data formatting | bytes 1048576
